TPU v7x, 32 devices: a whole 2x2x4 slice. The times are simulated.
32 devices in a mesh: sp: 4 (over y, x), dp: 8 (over z, core).
Axes of the slice: x: 2, y: 2, z: 4, core: 2. Of those that a mesh axis runs over, the one named last changes fastest.
Arguments:
- tokens: bfloat16 [8, 640, 2048], P('dp', 'sp'), may hold values from -42 to 42
- query_weight: bfloat16 [2048, 1024], P('dp'), may hold values from -1 to 1
- key_weight: bfloat16 [2048, 1024], P('dp'), may hold values from -1 to 1
- values: bfloat16 [8, 640, 1024], P('dp', 'sp'), may hold values from -6 to 6
- lambdas: float32 [16], replicated, may hold values from 0.3 to 0.8
- out_grad: bfloat16 [8, 640, 1024], P('dp', 'sp'), may hold values from -6 to 6
Outputs:
- tokens_grad: bfloat16 [8, 640, 2048], P('dp', 'sp')
- values_grad: bfloat16 [8, 640, 1024], P('dp', 'sp')
- query_weight_grad: float32 [2048, 1024], P('dp')
- key_weight_grad: float32 [2048, 1024], P('dp')
All inputs are finite; a program needn't handle non-finite values.
Results may differ from a plain program's by a relative error of at most 0.029.
The roundings to bfloat16 on the way count: a program that leaves them out, or rounds other values in their place, can miss the bound.
Values may be sent and summed in bfloat16 or wider, within the bound.
A program may use at most 128 MiB of HBM per device.

v0:
```python
import functools
import math

import jax
import jax.numpy as jnp
from jax import lax
from jax.experimental import pallas as pl
from jax.experimental.pallas import tpu as pltpu
from jax.sharding import PartitionSpec as P

DQK = 32
NORM_EPS = 0.1
THETA = 10000.0
F32 = jnp.float32
BF16 = jnp.bfloat16


def dot(a, b, ca=1, cb=0):
    return lax.dot_general(a, b, (((ca,), (cb,)), ((), ())), preferred_element_type=F32)


def rotation_tables(seq_length):
    half = DQK // 2
    freqs = jnp.exp(-math.log(THETA) * jnp.arange(half, dtype=F32) / half)
    angles = freqs[:, None] * jnp.arange(seq_length, dtype=jnp.int32).astype(F32)[None, :]
    return jnp.cos(angles), jnp.sin(angles)


def rotate_rows(x, cos, sin):
    half = DQK // 2
    parts = []
    for g in range(x.shape[0] // DQK):
        a = x[g * DQK : g * DQK + half]
        b = x[g * DQK + half : (g + 1) * DQK]
        parts += [a * cos - b * sin, b * cos + a * sin]
    return jnp.concatenate(parts, axis=0)


def attention_kernel(heads, lam_ref, cos_ref, sin_ref, qk_in, vog_ref, back_ref, rows_ref, dv_ref,
                     qk_ref, vt_s, ogt_s, dvt_s, dk_s):
    seq = cos_ref.shape[1]
    qc = qk_ref.shape[0] // 2
    hw = qc // heads
    ve = vog_ref.shape[2] // heads
    qk_ref[...] = qk_in[...].T
    inv_root = 1.0 / math.sqrt(DQK)
    vt_s[...] = vog_ref[0].T
    ogt_s[...] = vog_ref[1].T
    step = 256

    def one_head(h, _):
        lam = lam_ref[lax.axis_index("sp") * heads + h]
        cos, sin = cos_ref[...], sin_ref[...]
        qrow = pl.multiple_of(h * hw, hw)
        vrow = pl.multiple_of(h * ve, ve)
        qt = rotate_rows(qk_ref[pl.ds(qrow, hw), :], cos, sin).astype(BF16)
        kt = rotate_rows(qk_ref[pl.ds(qc + qrow, hw), :], cos, sin).astype(BF16)
        k = kt.T
        vt = vt_s[pl.ds(vrow, ve), :]
        v = vt.T
        zero_half = jnp.zeros((DQK, step), BF16)
        dk_s[...] = jnp.zeros_like(dk_s)
        dvt_s[pl.ds(vrow, ve), :] = jnp.zeros((ve, seq), F32)
        for t0 in range(0, seq, step):
            end = min(t0 + step, seq)
            tb = end - t0
            zh = zero_half[:, :tb]
            q_b = qt[:, t0:end]
            mask = lax.broadcasted_iota(jnp.int32, (tb, tb), 0) <= lax.broadcasted_iota(
                jnp.int32, (tb, tb), 1
            )
            probs = []
            for m in range(2):
                half_q = q_b[m * DQK : (m + 1) * DQK]
                rhs = jnp.concatenate([half_q, zh] if m == 0 else [zh, half_q], axis=0)
                s = dot(k[:end], rhs) * inv_root
                diag = jnp.where(mask, s[t0:], -jnp.inf)
                s = jnp.concatenate([s[:t0], diag], axis=0) if t0 else diag
                e = jnp.exp(s - jnp.max(s, axis=0, keepdims=True))
                probs.append(e * (1.0 / jnp.sum(e, axis=0, keepdims=True)))
            p1, p2 = probs
            mix = (p1 - lam * p2).astype(BF16)
            ho = dot(vt[:, :end], mix)
            inv = lax.rsqrt(jnp.mean(ho * ho, axis=0, keepdims=True) + NORM_EPS)
            og = ogt_s[pl.ds(vrow, ve), t0:end].astype(F32)
            ob = (inv * og - inv * inv * inv * ho * jnp.mean(og * ho, axis=0, keepdims=True)).astype(BF16)
            mg = dot(v[:end], ob) * inv_root
            g1 = (p1 * (mg - jnp.sum(mg * p1, axis=0, keepdims=True))).astype(BF16)
            g2 = ((-lam * p2) * (mg - jnp.sum(mg * p2, axis=0, keepdims=True))).astype(BF16)
            dvt_s[pl.ds(vrow, ve), :end] += dot(ob, mix, 1, 1)
            dq = jnp.concatenate([dot(kt[:DQK, :end], g1), dot(kt[DQK:, :end], g2)], axis=0)
            back_ref[pl.ds(qrow, hw), t0:end] = rotate_rows(dq, cos[:, t0:end], -sin[:, t0:end]).astype(BF16)
            dk_s[:DQK, :end] += dot(q_b[:DQK], g1, 1, 1)
            dk_s[DQK:, :end] += dot(q_b[DQK:], g2, 1, 1)
        back_ref[pl.ds(qc + qrow, hw), :] = rotate_rows(dk_s[...], cos, -sin).astype(BF16)
        return 0

    lax.fori_loop(0, heads, one_head, 0)
    dv_ref[...] = dvt_s[...].T.astype(BF16)
    rows_ref[...] = back_ref[...].T


def attention(qk, vog, lam, cos, sin, heads):
    seq, qk_cols = qk.shape
    vc = vog.shape[2]
    vm = pl.BlockSpec(memory_space=pltpu.VMEM)
    return pl.pallas_call(
        functools.partial(attention_kernel, heads),
        out_shape=(
            jax.ShapeDtypeStruct((qk_cols, seq), BF16),
            jax.ShapeDtypeStruct((seq, qk_cols), BF16),
            jax.ShapeDtypeStruct((seq, vc), BF16),
        ),
        in_specs=[pl.BlockSpec(memory_space=pltpu.SMEM)] + [vm] * 4,
        out_specs=(vm, vm, vm),
        scratch_shapes=[
            pltpu.VMEM((qk_cols, seq), F32),
            pltpu.VMEM((vc, seq), BF16),
            pltpu.VMEM((vc, seq), BF16),
            pltpu.VMEM((vc, seq), F32),
            pltpu.VMEM((qk_cols // heads // 2, seq), F32),
        ],
        compiler_params=pltpu.CompilerParams(vmem_limit_bytes=60 * 1024 * 1024),
        name="attn",
    )(lam, cos, sin, qk, vog)


def sender(src, dst, ssem, rsem, device):
    return pltpu.make_async_remote_copy(
        src_ref=src, dst_ref=dst, send_sem=ssem, recv_sem=rsem,
        device_id=device, device_id_type=pl.DeviceIdType.MESH,
    )


def places(sp, dp):
    me, mine = lax.axis_index("sp"), lax.axis_index("dp")
    z, core = mine // 2, lax.rem(mine, 2)
    nz = dp // 2
    if sp == 4:
        peers = [me + 1 - 2 * lax.rem(me, 2), lax.rem(me + 2, 4), 3 - me]
        froms = peers
    else:
        peers = [lax.rem(me + d, sp) for d in range(1, sp)]
        froms = [lax.rem(me + sp - d, sp) for d in range(1, sp)]
    z_to = [lax.rem(z + i, nz) * 2 for i in range(1, nz)]
    z_from = [lax.rem(z + nz - i, nz) * 2 for i in range(1, nz)]
    return me, mine, z, core, peers, froms, z_to, z_from


def greet(me, mine, core, peers, z_to):
    barrier = pltpu.get_barrier_semaphore()
    where = [(p, mine) for p in peers] + [(me, zt + core) for zt in z_to] + [(me, mine + 1 - 2 * core)]
    for device in where:
        pl.semaphore_signal(barrier, inc=1, device_id=device, device_id_type=pl.DeviceIdType.MESH)
    pl.semaphore_wait(barrier, len(where))


def gather_kernel(sp, dp, tok_ref, v_ref, og_ref, wq_ref, wk_ref, tok_all, vog_all, w_all, qk_ref,
                  vog_ref, tok_ss, tok_rs, vog_ss, vog_rs, w_ss, w_rs, sib_ss, sib_rs):
    me, mine, z, core, peers, froms, z_to, z_from = places(sp, dp)
    rows, wr = tok_ref.shape[0], wq_ref.shape[0]
    sib = (me, mine + 1 - 2 * core)

    def trow(i, start=0, size=rows):
        return pl.ds(pl.multiple_of(i * rows + start, 16), size)

    def wrow(i):
        return pl.ds(pl.multiple_of(i * wr, wr), wr)

    vc, qc = v_ref.shape[1] // sp, wq_ref.shape[1] // sp
    for s in range(sp):
        vog_ref[s, 0] = v_ref[:, s * vc : (s + 1) * vc]
        vog_ref[s, 1] = og_ref[:, s * vc : (s + 1) * vc]

        @pl.when(me == s)
        def _():
            w_all[wrow(mine), :qc] = wq_ref[:, s * qc : (s + 1) * qc]
            w_all[wrow(mine), qc:] = wk_ref[:, s * qc : (s + 1) * qc]

    tok_all[trow(me), :] = tok_ref[...]
    greet(me, mine, core, peers, z_to)
    w_ref = w_all.at[wrow(mine)]
    sends = []

    def go(copy):
        copy.start()
        sends.append(copy)
        return copy

    wz = [go(sender(w_ref, w_all.at[wrow(mine)], w_ss.at[i], w_rs.at[i], (me, zt + core)))
          for i, zt in enumerate(z_to)]
    ws = [go(sender(w_ref, w_all.at[wrow(mine)], sib_ss.at[0], sib_rs.at[0], sib))]
    half = rows // 2
    if sp == 4:
        def piece(p, h, k):
            r = trow(me, h * half, half)
            return go(sender(tok_ref.at[pl.ds(h * half, half)], tok_all.at[r], tok_ss.at[k], tok_rs.at[k], (p, mine)))

        x0, y1 = piece(peers[0], 0, 0), piece(peers[1], 1, 1)
        x1, y0 = piece(peers[0], 1, 2), piece(peers[1], 0, 3)
    else:
        tk = [go(sender(tok_ref, tok_all.at[trow(me)], tok_ss.at[i], tok_rs.at[i], (p, mine)))
              for i, p in enumerate(peers)]
    vg = [go(sender(vog_ref.at[p], vog_all.at[:, trow(me)], vog_ss.at[i], vog_rs.at[i], (p, mine)))
          for i, p in enumerate(peers)]
    vog_all[:, trow(me), :] = vog_ref[me]
    if sp == 4:
        x0.wait_recv()
        f0 = trow(peers[0], 0, half)
        d0 = go(sender(tok_all.at[f0], tok_all.at[f0], tok_ss.at[4], tok_rs.at[4], (peers[1], mine)))
        y1.wait_recv()
        f1 = trow(peers[1], half, half)
        d1 = go(sender(tok_all.at[f1], tok_all.at[f1], tok_ss.at[5], tok_rs.at[5], (peers[0], mine)))
        arrivals = [[x1], [y0], [d0, d1]]
    else:
        arrivals = [[c] for c in tk]
    for i, zf in enumerate(z_from):
        wz[i].wait_recv()
        r = wrow(zf + core)
        ws.append(go(sender(w_all.at[r], w_all.at[r], sib_ss.at[i + 1], sib_rs.at[i + 1], sib)))
    for c in ws:
        c.wait_recv()
    qk_ref[trow(me), :] = dot(tok_ref[...], w_all[...])
    for f, copies in zip(froms, arrivals):
        for c in copies:
            c.wait_recv()
        qk_ref[trow(f), :] = dot(tok_all[trow(f), :], w_all[...])
    for c in vg:
        c.wait_recv()
    for c in sends:
        c.wait_send()


def gather(tok, v, og, wq, wk, sp, dp):
    rows, width = tok.shape
    vc, wr, cols = v.shape[1] // sp, wq.shape[0], 2 * wq.shape[1] // sp
    vm = pl.BlockSpec(memory_space=pltpu.VMEM)
    dma = pltpu.SemaphoreType.DMA
    nt = 6 if sp == 4 else sp - 1
    nz = dp // 2
    return pl.pallas_call(
        functools.partial(gather_kernel, sp, dp),
        out_shape=(
            jax.ShapeDtypeStruct((rows * sp, width), BF16),
            jax.ShapeDtypeStruct((2, rows * sp, vc), BF16),
            jax.ShapeDtypeStruct((wr * dp, cols), BF16),
            jax.ShapeDtypeStruct((rows * sp, cols), F32),
        ),
        in_specs=[vm] * 5,
        out_specs=(vm,) * 4,
        scratch_shapes=[pltpu.VMEM((sp, 2, rows, vc), BF16), dma((nt,)), dma((nt,)), dma((sp - 1,)), dma((sp - 1,)),
                        dma((nz - 1,)), dma((nz - 1,)), dma((nz,)), dma((nz,))],
        compiler_params=pltpu.CompilerParams(
            vmem_limit_bytes=60 * 1024 * 1024, collective_id=0, has_side_effects=True
        ),
        name="gather",
    )(tok, v, og, wq, wk)


def scatter_kernel(sp, dp, back_t, back_m, tok_all, w_all, dv, tg_out, dv_out, qg, kg,
                   tbuf, trecv, tacc, dvr, sib_s, sib_r, wz_s, wz_r, wacc, wg_s, wg_r,
                   t_ss, t_rs, d_ss, d_rs, s_ss, s_rs, z_ss, z_rs, g_ss, g_rs):
    me, mine, z, core, peers, froms, z_to, z_from = places(sp, dp)
    nz = dp // 2
    rows, wr = tg_out.shape[0], qg.shape[0]
    vc = dv.shape[1]
    qc = w_all.shape[1] // 2
    sib = (me, mine + 1 - 2 * core)
    greet(me, mine, core, peers, z_to)
    sends = []

    def go(copy):
        copy.start()
        sends.append(copy)
        return copy

    def trow(i):
        return pl.ds(pl.multiple_of(i * rows, 16), rows)

    def weight_part(owner):
        return dot(back_t[...], tok_all[:, pl.ds(pl.multiple_of(owner * wr, wr), wr)])

    def token_part(p):
        return dot(back_m[trow(p), :], w_all[...], 1, 1)

    def send_tokens(i):
        tbuf[i] = token_part(peers[i]).astype(BF16)
        return go(sender(tbuf.at[i], trecv.at[i], t_ss.at[i], t_rs.at[i], (peers[i], mine)))

    targets = z_to + [z * 2]
    half = rows // 2
    lo, hi = pl.ds(0, half), pl.ds(half, half)
    tg = []

    def hop(i, dst, part, k, to):
        return go(sender(tbuf.at[i, part], trecv.at[dst, part], t_ss.at[k], t_rs.at[k], (peers[to], mine)))

    if sp == 4:
        tbuf[2] = token_part(peers[2]).astype(BF16)
        via_x, via_y = hop(2, 2, lo, 0, 0), hop(2, 2, hi, 1, 1)
    else:
        tg.append(send_tokens(0))
    sb = []
    for i, zt in enumerate(targets):
        sib_s[i] = weight_part(zt + 1 - core).astype(BF16)
        sb.append(go(sender(sib_s.at[i], sib_r.at[i], s_ss.at[i], s_rs.at[i], sib)))
    zs = []
    for i, zt in enumerate(targets):
        part = weight_part(zt + core)
        sb[i].wait_recv()
        part = part + sib_r[i].astype(F32)
        if i < nz - 1:
            wz_s[i] = part.astype(BF16)
            zs.append(go(sender(wz_s.at[i], wz_r.at[i], z_ss.at[i], z_rs.at[i], (me, zt + core))))
        else:
            wacc[...] = part
    if sp == 4:
        part = token_part(peers[0])
        tbuf[0, lo] = part[:half].astype(BF16)
        x_lo = hop(0, 0, lo, 2, 0)
        tacc[hi] = part[half:]
        part = token_part(peers[1])
        tbuf[1, hi] = part[half:].astype(BF16)
        y_hi = hop(1, 1, hi, 3, 1)
        tacc[lo] = part[:half]
        via_x.wait_recv()
        tbuf[1, lo] = (tacc[lo] + trecv[2, lo].astype(F32)).astype(BF16)
        y_lo = hop(1, 1, lo, 4, 1)
        via_y.wait_recv()
        tbuf[0, hi] = (tacc[hi] + trecv[2, hi].astype(F32)).astype(BF16)
        x_hi = hop(0, 0, hi, 5, 0)
        tg = [x_lo, x_hi, y_lo, y_hi]
    else:
        for i in range(1, sp - 1):
            tg.append(send_tokens(i))
    dvc = [go(sender(dv.at[trow(p)], dvr.at[me], d_ss.at[i], d_rs.at[i], (p, mine)))
           for i, p in enumerate(peers)]
    dvr[me] = dv[trow(me), :]
    tacc[...] = token_part(me)
    for i in range(nz - 1):
        zs[i].wait_recv()
        wacc[...] += wz_r[i].astype(F32)
    total = wacc[...].T.astype(BF16)
    wg_s[...] = total
    wg_r[me] = total
    wh = wr // 2
    if sp == 4:
        def piece(p, h, k):
            r = pl.ds(h * wh, wh)
            return go(sender(wg_s.at[r], wg_r.at[me, r], g_ss.at[k], g_rs.at[k], (p, mine)))

        def forward(f, h, k, p):
            r = pl.ds(h * wh, wh)
            return go(sender(wg_r.at[f, r], wg_r.at[f, r], g_ss.at[k], g_rs.at[k], (p, mine)))

        gx0, gy1 = piece(peers[0], 0, 0), piece(peers[1], 1, 1)
        gx1, gy0 = piece(peers[0], 1, 2), piece(peers[1], 0, 3)
        gx0.wait_recv()
        gd0 = forward(peers[0], 0, 4, peers[1])
        gy1.wait_recv()
        gd1 = forward(peers[1], 1, 5, peers[0])
        gs = [gx1, gy0, gd0, gd1]
    else:
        gs = [go(sender(wg_s, wg_r.at[me], g_ss.at[i], g_rs.at[i], (p, mine))) for i, p in enumerate(peers)]
    for c in tg:
        c.wait_recv()
    for i in range(2 if sp == 4 else sp - 1):
        tacc[...] += trecv[i].astype(F32)
    tg_out[...] = tacc[...].astype(BF16)
    for c in dvc:
        c.wait_recv()
    for s in range(sp):
        dv_out[:, s * vc : (s + 1) * vc] = dvr[s]
    for c in gs:
        c.wait_recv()
    for s in range(sp):
        qg[:, s * qc : (s + 1) * qc] = wg_r[s, :, :qc]
        kg[:, s * qc : (s + 1) * qc] = wg_r[s, :, qc:]
    for c in sends:
        c.wait_send()


def scatter(back_t, back_m, tok_all, w_all, dv, sp, dp):
    seq, width = tok_all.shape
    rows, wr = seq // sp, width // dp
    cols = w_all.shape[1]
    vc = dv.shape[1]
    nz = dp // 2
    vm = pl.BlockSpec(memory_space=pltpu.VMEM)
    dma = pltpu.SemaphoreType.DMA
    nt = 6 if sp == 4 else sp - 1
    return pl.pallas_call(
        functools.partial(scatter_kernel, sp, dp),
        out_shape=(
            jax.ShapeDtypeStruct((rows, width), BF16),
            jax.ShapeDtypeStruct((rows, vc * sp), BF16),
            jax.ShapeDtypeStruct((wr, cols // 2 * sp), BF16),
            jax.ShapeDtypeStruct((wr, cols // 2 * sp), BF16),
        ),
        in_specs=[vm] * 5,
        out_specs=(vm,) * 4,
        scratch_shapes=[
            pltpu.VMEM((sp - 1, rows, width), BF16),
            pltpu.VMEM((sp - 1, rows, width), BF16),
            pltpu.VMEM((rows, width), F32),
            pltpu.VMEM((sp, rows, vc), BF16),
            pltpu.VMEM((nz, cols, wr), BF16),
            pltpu.VMEM((nz, cols, wr), BF16),
            pltpu.VMEM((nz - 1, cols, wr), BF16),
            pltpu.VMEM((nz - 1, cols, wr), BF16),
            pltpu.VMEM((cols, wr), F32),
            pltpu.VMEM((wr, cols), BF16),
            pltpu.VMEM((sp, wr, cols), BF16),
            dma((nt,)), dma((nt,)), dma((sp - 1,)), dma((sp - 1,)), dma((nz,)), dma((nz,)),
            dma((nz - 1,)), dma((nz - 1,)), dma((nt,)), dma((nt,)),
        ],
        compiler_params=pltpu.CompilerParams(
            vmem_limit_bytes=62 * 1024 * 1024, collective_id=1, has_side_effects=True
        ),
        name="scatter",
    )(back_t, back_m, tok_all, w_all, dv)


def body(tokens, query_weight, key_weight, values, lambdas, out_grad):
    sp = lax.axis_size("sp")
    dp = lax.axis_size("dp")
    rows = tokens.shape[1]
    heads = lambdas.shape[0] // sp
    cos, sin = rotation_tables(rows * sp)
    tok_all, vog_all, w_all, qk = gather(
        tokens[0], values[0], out_grad[0], query_weight, key_weight, sp, dp
    )
    back_t, back_m, dv = attention(qk, vog_all, lambdas, cos, sin, heads)
    tokens_grad, values_grad, qg, kg = scatter(back_t, back_m, tok_all, w_all, dv, sp, dp)
    factor = 1.0 / math.sqrt(dp * rows * sp)
    return tokens_grad[None], values_grad[None], qg.astype(F32) * factor, kg.astype(F32) * factor


def solution(mesh):
    x = P("dp", "sp", None)
    w = P("dp", None)
    return jax.shard_map(
        body, mesh=mesh, in_specs=(x, w, w, x, P(), x), out_specs=(x, x, w, w), check_vma=False
    )
```

profile of v0, /device:TPU:0, one launch (start us, length us, event | category | flops | bytes accessed | tf_op | source)
XLA Modules:
  0.0 104.6 jit_solution(10232858303163860588)
XLA Ops:
  0.7 0.9 multiply_sine_fusion
  1.5 40.5 %gather.1 = (bf16[640,2048]{1,0:T(8,128)(2,1)}, bf16[2,640,256]{2,1,0:T(8,128)(2,1)}, bf16[2048,512]{1,0:T(8,128)(2,1)}, f32[640,512]{1,0:T(8,128)}) custom-call(bf16[160,2048]{1,0:T(8,128)(2,1)} %bitcast.5, bf16[160,1024]{1,0:T(8,128)(2,1)} %bitcast.7, bf16[160,1024]{1,0:T(8,128)(2,1)} %bitcast.8, bf16[256,1024]{1,0:T(8,128)(2,1)} %wq_ref.1, ...), custom_call_target="tpu_custom_call" | custom-call | tf_op jit(solution)/shard_map/gather/pallas_call | solution.py:241
  42.0 16.8 %attn.1 = (bf16[512,640]{1,0:T(8,128)(2,1)}, bf16[640,512]{1,0:T(8,128)(2,1)}, bf16[640,256]{1,0:T(8,128)(2,1)}) custom-call(f32[16]{0:T(128)} %lam_ref.1, f32[16,640]{1,0:T(8,128)} %get-tuple-element.27.cos_ref, f32[16,640]{1,0:T(8,128)} %get-tuple-element.26.sin_ref, f32[640,512]{1,0:T(8,128)} %get-tuple-element.15.qk_in, ...), custom_call_target="tpu_custom_call" | custom-call | tf_op jit(solution)/shard_map/attn/pallas_call | solution.py:107
  58.8 41.4 %scatter.1 = (bf16[160,2048]{1,0:T(8,128)(2,1)}, bf16[160,1024]{1,0:T(8,128)(2,1)}, bf16[256,1024]{1,0:T(8,128)(2,1)}, bf16[256,1024]{1,0:T(8,128)(2,1)}) custom-call(bf16[512,640]{1,0:T(8,128)(2,1)} %get-tuple-element.17.back_t, bf16[640,512]{1,0:T(8,128)(2,1)} %get-tuple-element.18.back_m, bf16[640,2048]{1,0:T(8,128)(2,1)} %get-tuple-element.19.tok_all, ...), custom_call_target="tpu_custom_call" | custom-call | tf_op jit(solution)/shard_map/scatter/pallas_call | solution.py:392
  100.2 0.0 copy-start
  100.2 0.0 copy-start.1
  100.2 2.9 %convert_multiply_fusion = (f32[256,1024]{1,0:T(8,128)}, f32[256,1024]{1,0:T(8,128)}) fusion(bf16[256,1024]{1,0:T(8,128)(2,1)} %get-tuple-element.25, bf16[256,1024]{1,0:T(8,128)(2,1)} %get-tuple-element.24), kind=kLoop, calls=%fused_computation | loop fusion | flops 1048576 | bytes 3145728 | tf_op jit(solution)/shard_map/mul | solution.py:436
  103.1 0.0 copy-done
  103.1 0.8 copy.12
  103.9 0.0 copy-done.1
  103.9 0.7 copy.13
  (2 shorter events, 0.0 us)
Async XLA Ops:
  100.2 2.9 %copy-start = (bf16[160,2048]{1,0:T(8,128)(2,1)S(1)}, bf16[160,2048]{1,0:T(8,128)(2,1)}, u32[]{:S(2)}) copy-start(bf16[160,2048]{1,0:T(8,128)(2,1)} %get-tuple-element.22) | copy-start | bytes 1966084
  100.2 3.7 %copy-start.1 = (bf16[160,1024]{1,0:T(8,128)(2,1)S(1)}, bf16[160,1024]{1,0:T(8,128)(2,1)}, u32[]{:S(2)}) copy-start(bf16[160,1024]{1,0:T(8,128)(2,1)} %get-tuple-element.23) | copy-start | bytes 983044
where the time goes:
time: 107 us; the launch traced here: 105 us
  Pallas kernels  98.6 us (92%)
  other arithmetic  3.75 us (4%)
  local copies, waits for them, and re-layouts  1.57 us (1%)
    pallas_call x1, Pallas kernels, scatter(): pl.pallas_call(functools.partial(scatter_kernel, sp, dp), out_shape=(jax....  41.4 us
    pallas_call x1, Pallas kernels, gather(): pl.pallas_call(functools.partial(gather_kernel, sp, dp), out_shape=(jax.S...  40.5 us
    pallas_call x1, Pallas kernels, attention(): pl.pallas_call(functools.partial(attention_kernel, heads), out_shape=(jax...  16.8 us
    mul x1, other arithmetic, body(): kg.astype(F32) * factor  2.88 us

commit v1 on v0

--- a/solution.py
+++ b/solution.py
@@ -421,12 +421,324 @@
     )(back_t, back_m, tok_all, w_all, dv)
 
 
+def head_pair(h0, lam_ref, cos, sin, qk, vt_s, ogt_s, dvt_s, dk_s, bt_s):
+    seq = cos.shape[1]
+    hw = 2 * DQK
+    ve = vt_s.shape[0] // 2
+    inv_root = 1.0 / math.sqrt(DQK)
+    step = 256
+    zero_half = jnp.zeros((DQK, step), BF16)
+    for hh in range(2):
+        lam = lam_ref[h0 + hh]
+        rows = slice(hh * hw, (hh + 1) * hw)
+        vr = slice(hh * ve, (hh + 1) * ve)
+        qt = rotate_rows(qk[0][rows], cos, sin).astype(BF16)
+        kt = rotate_rows(qk[1][rows], cos, sin).astype(BF16)
+        k = kt.T
+        vt = vt_s[vr, :]
+        v = vt.T
+        for t0 in range(0, seq, step):
+            end = min(t0 + step, seq)
+            tb = end - t0
+            zh = zero_half[:, :tb]
+            q_b = qt[:, t0:end]
+            mask = lax.broadcasted_iota(jnp.int32, (tb, tb), 0) <= lax.broadcasted_iota(
+                jnp.int32, (tb, tb), 1
+            )
+            probs = []
+            for m in range(2):
+                half_q = q_b[m * DQK : (m + 1) * DQK]
+                rhs = jnp.concatenate([half_q, zh] if m == 0 else [zh, half_q], axis=0)
+                s = dot(k[:end], rhs) * inv_root
+                diag = jnp.where(mask, s[t0:], -jnp.inf)
+                s = jnp.concatenate([s[:t0], diag], axis=0) if t0 else diag
+                e = jnp.exp(s - jnp.max(s, axis=0, keepdims=True))
+                probs.append(e * (1.0 / jnp.sum(e, axis=0, keepdims=True)))
+            p1, p2 = probs
+            mix = (p1 - lam * p2).astype(BF16)
+            ho = dot(vt[:, :end], mix)
+            inv = lax.rsqrt(jnp.mean(ho * ho, axis=0, keepdims=True) + NORM_EPS)
+            og = ogt_s[vr, t0:end].astype(F32)
+            ob = (inv * og - inv * inv * inv * ho * jnp.mean(og * ho, axis=0, keepdims=True)).astype(BF16)
+            mg = dot(v[:end], ob) * inv_root
+            g1 = (p1 * (mg - jnp.sum(mg * p1, axis=0, keepdims=True))).astype(BF16)
+            g2 = ((-lam * p2) * (mg - jnp.sum(mg * p2, axis=0, keepdims=True))).astype(BF16)
+            dvd = dot(ob, mix, 1, 1)
+            dkd = jnp.concatenate([dot(q_b[:DQK], g1, 1, 1), dot(q_b[DQK:], g2, 1, 1)], axis=0)
+            if t0:
+                dvd = jnp.concatenate([dvt_s[vr, :t0] + dvd[:, :t0], dvd[:, t0:]], axis=1)
+                dkd = jnp.concatenate([dk_s[rows, :t0] + dkd[:, :t0], dkd[:, t0:]], axis=1)
+            dvt_s[vr, :end] = dvd
+            dk_s[rows, :end] = dkd
+            dq = jnp.concatenate([dot(kt[:DQK, :end], g1), dot(kt[DQK:, :end], g2)], axis=0)
+            bt_s[rows, t0:end] = rotate_rows(dq, cos[:, t0:end], -sin[:, t0:end]).astype(BF16)
+        bt_s[2 * hw + hh * hw : 2 * hw + (hh + 1) * hw, :] = rotate_rows(dk_s[rows, :], cos, -sin).astype(BF16)
+
+
+def fused_kernel(sp, dp, pairs, factor, lam_ref, cos_ref, sin_ref, tok_ref, v_ref, og_ref, wq_ref, wk_ref,
+                 tg_out, dv_out, qg, kg,
+                 tok_all, w1, w2, qk_s, vog_src, vog_all, vt_s, ogt_s, dvt_s, dk_s, bt_s, back_m, back_x,
+                 dv_s, dvr, sib_s, sib_r, wz_s, wz_r, wacc, wg_r, tbuf, trecv,
+                 tok_ss, tok_rs, vog_ss, vog_rs, z_ss, z_rs, s_ss, s_rs, bx_ss, bx_rs, dv_ss, dv_rs,
+                 c_ss, c_rs, g_ss, g_rs, ag_ss, ag_rs, ty_ss, ty_rs):
+    me, mine, z, core, peers, froms, z_to, z_from = places(sp, dp)
+    nz = dp // 2
+    rows, wr = tok_ref.shape[0], wq_ref.shape[0]
+    half = rows // 2
+    width = tok_ref.shape[1]
+    pw = 128
+    cw = pairs * pw
+    sib = (me, mine + 1 - 2 * core)
+    xp, yp = (peers[0], mine), (peers[1], mine)
+
+    def trow(i, start=0, size=rows):
+        return pl.ds(pl.multiple_of(i * rows + start, 16), size)
+
+    def wrow(i):
+        return pl.ds(pl.multiple_of(i * wr, wr), wr)
+
+    def lanes(i, size):
+        return pl.ds(pl.multiple_of(i * size, size), size)
+
+    sends = []
+
+    def go(copy, cond=None):
+        if cond is None:
+            copy.start()
+        else:
+            pl.when(cond)(copy.start)
+        sends.append((copy, cond))
+        return copy
+
+    for w, who in ((w1, me), (w2, peers[0])):
+        for j in range(pairs):
+            src = lanes(who * pairs + j, pw)
+            w[wrow(mine), 2 * j * pw : (2 * j + 1) * pw] = wq_ref[:, src]
+            w[wrow(mine), (2 * j + 1) * pw : (2 * j + 2) * pw] = wk_ref[:, src]
+    for s in range(sp):
+        for j in range(pairs):
+            c = (s * pairs + j) * pw
+            vog_src[s, j, 0] = v_ref[:, c : c + pw]
+            vog_src[s, j, 1] = og_ref[:, c : c + pw]
+    tok_all[trow(me), :] = tok_ref[...]
+    greet(me, mine, core, peers, z_to)
+
+    def z_start(w, k):
+        r = w.at[wrow(mine)]
+        for n, d in enumerate((2, -2, 1, -1)):
+            cond = (z + d < nz) if d > 0 else (z + d >= 0)
+            go(sender(r, r, z_ss.at[k, n], z_rs.at[k, z], (me, (z + d) * 2 + core)), cond)
+        go(sender(r, r, s_ss.at[k, z], s_rs.at[k, z], sib))
+
+    far = lax.rem(z + 2, nz)
+    order = [far, z + 1 - 2 * lax.rem(z, 2), nz - 1 - z]
+
+    def z_step(w, k, i):
+        src = order[i]
+        r = w.at[wrow(2 * src + core)]
+        sender(r, r, z_ss.at[k, 0], z_rs.at[k, src], sib).wait_recv()
+        go(sender(r, r, s_ss.at[k, src], s_rs.at[k, src], sib))
+        if i == 0:
+            inner = jnp.logical_and(z > 0, z < nz - 1)
+            go(sender(r, r, z_ss.at[k, 4], z_rs.at[k, src], (me, (z - 1) * (nz - 1) * 2 + core)), inner)
+
+    def z_sib(w, k):
+        for src in [z] + order:
+            r = w.at[wrow(2 * src + 1 - core)]
+            sender(r, r, s_ss.at[k, 0], s_rs.at[k, src], sib).wait_recv()
+
+    def piece(p, h, k):
+        r = trow(me, h * half, half)
+        return go(sender(tok_ref.at[pl.ds(h * half, half)], tok_all.at[r], tok_ss.at[k], tok_rs.at[k], p))
+
+    z_start(w1, 0)
+    x0, y1 = piece(xp, 0, 0), piece(yp, 1, 1)
+    x1, y0 = piece(xp, 1, 2), piece(yp, 0, 3)
+    x0.wait_recv()
+    f0 = trow(peers[0], 0, half)
+    d0 = go(sender(tok_all.at[f0], tok_all.at[f0], tok_ss.at[4], tok_rs.at[4], yp))
+    y1.wait_recv()
+    f1 = trow(peers[1], half, half)
+    d1 = go(sender(tok_all.at[f1], tok_all.at[f1], tok_ss.at[5], tok_rs.at[5], xp))
+    for j in range(pairs):
+        for i, p in enumerate(peers):
+            go(sender(vog_src.at[p, j], vog_all.at[j, :, trow(me)], vog_ss.at[j, i], vog_rs.at[j, i], (p, mine)))
+        vog_all[j, :, trow(me), :] = vog_src[me, j]
+    for i in range(3):
+        z_step(w1, 0, i)
+    z_start(w2, 1)
+    z_sib(w1, 0)
+    qk_s[trow(me), :] = dot(tok_ref[...], w1[...])
+    for f, copies in zip(froms, [[x1], [y0], [d0, d1]]):
+        for c in copies:
+            c.wait_recv()
+        qk_s[trow(f), :] = dot(tok_all[trow(f), :], w1[...])
+
+    targets = z_to + [z]
+    cos, sin = cos_ref[...], sin_ref[...]
+
+    def one_pair(j):
+        qk = [qk_s[:, (2 * j + n) * pw : (2 * j + n + 1) * pw].T for n in range(2)]
+        for i, p in enumerate(peers):
+            r = vog_all.at[j, :, trow(p)]
+            sender(vog_src.at[p, j], r, vog_ss.at[j, i], vog_rs.at[j, i], (p, mine)).wait_recv()
+        vt_s[...] = vog_all[j, 0].T
+        ogt_s[...] = vog_all[j, 1].T
+        head_pair(me * 2 * pairs + 2 * j, lam_ref, cos, sin, qk, vt_s, ogt_s, dvt_s, dk_s, bt_s)
+        back_m[j] = bt_s[...].T
+        for b, p in enumerate((peers[0], peers[2])):
+            go(sender(back_m.at[j, trow(p)], back_x.at[j, b], bx_ss.at[j, b], bx_rs.at[j, b], xp))
+        dv_s[j] = dvt_s[...].T.astype(BF16)
+        for i, p in enumerate(peers):
+            go(sender(dv_s.at[j, trow(p)], dvr.at[me, j], dv_ss.at[j, i], dv_rs.at[j, i], (p, mine)))
+        dvr[me, j] = dv_s[j, trow(me), :]
+
+        def weight_part(owner):
+            return dot(bt_s[...], tok_all[:, lanes(owner, wr)])
+
+        for i, zt in enumerate(targets):
+            zz = zt // 2 if i < nz - 1 else zt
+            sib_s[j, i] = weight_part(2 * zz + 1 - core).astype(BF16)
+            go(sender(sib_s.at[j, i], sib_r.at[j, i], c_ss.at[j, i], c_rs.at[j, i], sib))
+        for i, zt in enumerate(targets):
+            zz = zt // 2 if i < nz - 1 else zt
+            part = weight_part(2 * zz + core)
+            sender(sib_s.at[j, i], sib_r.at[j, i], c_ss.at[j, i], c_rs.at[j, i], sib).wait_recv()
+            part = part + sib_r[j, i].astype(F32)
+            if i < nz - 1:
+                wz_s[j, i] = part.astype(BF16)
+                go(sender(wz_s.at[j, i], wz_r.at[j, i], g_ss.at[j, i], g_rs.at[j, i], (me, zt + core)))
+            else:
+                wacc[j] = part
+
+    for j in range(pairs):
+        one_pair(j)
+        if j == 0:
+            z_step(w2, 1, 0)
+            z_step(w2, 1, 1)
+    z_step(w2, 1, 2)
+    z_sib(w2, 1)
+
+    nc = 4
+    cols = width // nc
+
+    def back_wait(b):
+        for j in range(pairs):
+            r = back_x.at[j, b]
+            sender(r, r, bx_ss.at[j, b], bx_rs.at[j, b], xp).wait_recv()
+
+    def token_part(who, b, c):
+        n = slice(c * cols, (c + 1) * cols)
+        out = None
+        for j in range(pairs):
+            k = slice(2 * j * pw, (2 * j + 2) * pw)
+            for lhs, w in ((back_m[j, trow(who), :], w1), (back_x[j, b], w2)):
+                part = dot(lhs, w[n, k], 1, 1)
+                out = part if out is None else out + part
+        return out
+
+    back_wait(1)
+    ty = []
+    for c in range(nc):
+        tbuf[c] = token_part(peers[1], 1, c).astype(BF16)
+        ty.append(go(sender(tbuf.at[c], trecv.at[c], ty_ss.at[c], ty_rs.at[c], yp)))
+    back_wait(0)
+
+    for j in range(pairs):
+        for i in range(nz - 1):
+            r = wz_r.at[j, i]
+            sender(r, r, g_ss.at[j, i], g_rs.at[j, i], sib).wait_recv()
+            wacc[j] += wz_r[j, i].astype(F32)
+        wg_r[me, j] = wacc[j].T.astype(BF16)
+        mine_r = wg_r.at[me, j]
+        go(sender(mine_r, mine_r, ag_ss.at[j, 0], ag_rs.at[j, 0], yp))
+        go(sender(mine_r, mine_r, ag_ss.at[j, 1], ag_rs.at[j, 1], xp))
+        r = wg_r.at[peers[1], j]
+        sender(r, r, ag_ss.at[j, 0], ag_rs.at[j, 0], yp).wait_recv()
+        go(sender(r, r, ag_ss.at[j, 2], ag_rs.at[j, 2], xp))
+    for c in range(nc):
+        part = token_part(me, 0, c)
+        ty[c].wait_recv()
+        tg_out[:, c * cols : (c + 1) * cols] = (part + trecv[c].astype(F32)).astype(BF16)
+    for j in range(pairs):
+        for i, p in enumerate(peers):
+            r = dvr.at[p, j]
+            sender(r, r, dv_ss.at[j, i], dv_rs.at[j, i], xp).wait_recv()
+        for s in range(sp):
+            c = (s * pairs + j) * pw
+            dv_out[:, c : c + pw] = dvr[s, j]
+    for j in range(pairs):
+        for i, p in ((1, peers[0]), (2, peers[2])):
+            r = wg_r.at[p, j]
+            sender(r, r, ag_ss.at[j, i], ag_rs.at[j, i], xp).wait_recv()
+        for s in range(sp):
+            c = (s * pairs + j) * pw
+            qg[:, c : c + pw] = wg_r[s, j, :, :pw].astype(F32) * factor
+            kg[:, c : c + pw] = wg_r[s, j, :, pw:].astype(F32) * factor
+    for c, cond in sends:
+        if cond is None:
+            c.wait_send()
+        else:
+            pl.when(cond)(c.wait_send)
+
+
+def fused(tok, v, og, wq, wk, lam, cos, sin, sp, dp):
+    rows, width = tok.shape
+    seq = rows * sp
+    wr = wq.shape[0]
+    nz = dp // 2
+    pw = 128
+    pairs = v.shape[1] // (sp * pw)
+    factor = 1.0 / math.sqrt(dp * seq)
+    vm = pl.BlockSpec(memory_space=pltpu.VMEM)
+    dma = pltpu.SemaphoreType.DMA
+    V = pltpu.VMEM
+    nc = 4
+    return pl.pallas_call(
+        functools.partial(fused_kernel, sp, dp, pairs, factor),
+        out_shape=(
+            jax.ShapeDtypeStruct((rows, width), BF16),
+            jax.ShapeDtypeStruct((rows, v.shape[1]), BF16),
+            jax.ShapeDtypeStruct((wr, wq.shape[1]), F32),
+            jax.ShapeDtypeStruct((wr, wq.shape[1]), F32),
+        ),
+        in_specs=[pl.BlockSpec(memory_space=pltpu.SMEM)] + [vm] * 7,
+        out_specs=(vm,) * 4,
+        scratch_shapes=[
+            V((seq, width), BF16), V((width, 2 * pairs * pw), BF16), V((width, 2 * pairs * pw), BF16),
+            V((seq, 2 * pairs * pw), F32), V((sp, pairs, 2, rows, pw), BF16), V((pairs, 2, seq, pw), BF16),
+            V((pw, seq), BF16), V((pw, seq), BF16), V((pw, seq), F32), V((pw, seq), F32), V((2 * pw, seq), BF16),
+            V((pairs, seq, 2 * pw), BF16), V((pairs, 2, rows, 2 * pw), BF16),
+            V((pairs, seq, pw), BF16), V((sp, pairs, rows, pw), BF16),
+            V((pairs, nz, 2 * pw, wr), BF16), V((pairs, nz, 2 * pw, wr), BF16),
+            V((pairs, nz - 1, 2 * pw, wr), BF16), V((pairs, nz - 1, 2 * pw, wr), BF16),
+            V((pairs, 2 * pw, wr), F32), V((sp, pairs, wr, 2 * pw), BF16),
+            V((nc, rows, width // nc), BF16), V((nc, rows, width // nc), BF16),
+            dma((6,)), dma((6,)), dma((pairs, sp - 1)), dma((pairs, sp - 1)),
+            dma((2, 5)), dma((2, nz)), dma((2, nz)), dma((2, nz)),
+            dma((pairs, 2)), dma((pairs, 2)), dma((pairs, sp - 1)), dma((pairs, sp - 1)),
+            dma((pairs, nz)), dma((pairs, nz)), dma((pairs, nz - 1)), dma((pairs, nz - 1)),
+            dma((pairs, 3)), dma((pairs, 3)), dma((nc,)), dma((nc,)),
+        ],
+        compiler_params=pltpu.CompilerParams(
+            vmem_limit_bytes=62 * 1024 * 1024, collective_id=2, has_side_effects=True
+        ),
+        name="fused",
+    )(lam, cos, sin, tok, v, og, wq, wk)
+
+
 def body(tokens, query_weight, key_weight, values, lambdas, out_grad):
     sp = lax.axis_size("sp")
     dp = lax.axis_size("dp")
     rows = tokens.shape[1]
     heads = lambdas.shape[0] // sp
     cos, sin = rotation_tables(rows * sp)
+    head_vec = values.shape[2] // lambdas.shape[0]
+    if sp == 4 and dp == 8 and heads % 2 == 0 and head_vec == 64 and rows * sp <= 640:
+        tg, dv, qg, kg = fused(
+            tokens[0], values[0], out_grad[0], query_weight, key_weight, lambdas, cos, sin, sp, dp
+        )
+        return tg[None], dv[None], qg, kg
     tok_all, vog_all, w_all, qk = gather(
         tokens[0], values[0], out_grad[0], query_weight, key_weight, sp, dp
     )

time: 107 us -> 104 us (0.972); the launches traced: 105 us -> 104 us
  local copies, waits for them, and re-layouts: 1.57 us -> 6.36 us
  other arithmetic: 3.75 us -> 0.87 us
  Pallas kernels: 98.6 us -> 96.3 us
    unnamed x6 -> x8, local copies, waits for them, and re-layouts: 1.57 us -> 6.36 us
    mul x1 -> x0, other arithmetic: 2.88 us -> none  [body(): kg.astype(F32) * factor]
    pallas_call x3 -> x1, Pallas kernels: 98.6 us -> 96.3 us  [fused(): pl.pallas_call(functools.partial(fused_kernel, sp, dp, pairs, factor), ou...]
where the time goes in v1:
time: 104 us
  Pallas kernels  96.3 us (93%)
  local copies, waits for them, and re-layouts  6.36 us (6%)
    pallas_call x1, Pallas kernels, fused(): pl.pallas_call(functools.partial(fused_kernel, sp, dp, pairs, factor), ou...  96.3 us
    unnamed x8, local copies, waits for them, and re-layouts  6.36 us

profile of v1, /device:TPU:0, one launch (start us, length us, event | category | flops | bytes accessed | tf_op | source)
XLA Modules:
  0.0 104.2 jit_solution(12481848585372819951)
XLA Ops:
  0.7 0.9 multiply_sine_fusion
  1.5 96.3 %fused.1 = (bf16[160,2048]{1,0:T(8,128)(2,1)}, bf16[160,1024]{1,0:T(8,128)(2,1)}, f32[256,1024]{1,0:T(8,128)}, f32[256,1024]{1,0:T(8,128)}) custom-call(f32[16]{0:T(128)} %lam_ref.1, f32[16,640]{1,0:T(8,128)} %get-tuple-element.13.cos_ref, f32[16,640]{1,0:T(8,128)} %get-tuple-element.12.sin_ref, bf16[160,2048]{1,0:T(8,128)(2,1)} %bitcast.6, ...), custom_call_target="tpu_custom_call" | custom-call | tf_op jit(solution)/shard_map/fused/pallas_call | solution.py:697
  97.8 0.0 copy-start.1
  97.8 2.1 %copy.14 = bf16[1,160,2048]{2,1,0:T(8,128)(2,1)} copy(bf16[1,160,2048]{2,1,0:T(8,128)(2,1)} %bitcast.5) | data formatting | bytes 1310720
  99.9 1.7 %copy.15 = bf16[1,160,1024]{2,1,0:T(8,128)(2,1)} copy(bf16[1,160,1024]{2,1,0:T(8,128)(2,1)} %bitcast.7) | data formatting | bytes 655360
  101.6 0.0 copy-done.1
  101.6 0.0 copy-start
  101.6 1.0 copy.16
  102.6 0.6 copy-done
  103.2 1.0 copy.17
  (2 shorter events, 0.0 us)
Async XLA Ops:
  97.8 3.8 %copy-start.1 = (f32[256,1024]{1,0:T(8,128)S(1)}, f32[256,1024]{1,0:T(8,128)}, u32[]{:S(2)}) copy-start(f32[256,1024]{1,0:T(8,128)} %get-tuple-element.20) | copy-start | bytes 3145732
  101.6 1.6 %copy-start = (f32[256,1024]{1,0:T(8,128)S(1)}, f32[256,1024]{1,0:T(8,128)}, u32[]{:S(2)}) copy-start(f32[256,1024]{1,0:T(8,128)} %get-tuple-element.21) | copy-start | bytes 3145732

commit v2 on v0

--- a/solution.py
+++ b/solution.py
@@ -3,6 +3,7 @@
 
 import jax
 import jax.numpy as jnp
+import numpy as np
 from jax import lax
 from jax.experimental import pallas as pl
 from jax.experimental.pallas import tpu as pltpu
@@ -421,11 +422,413 @@
     )(back_t, back_m, tok_all, w_all, dv)
 
 
+def position_tables(seq_length):
+    half = DQK // 2
+    freqs = np.exp(np.float32(-math.log(THETA)) * np.arange(half, dtype=np.float32) / np.float32(half)).astype(np.float32)
+    angles = freqs[:, None] * np.arange(seq_length, dtype=np.float32)[None, :]
+    wide = angles.astype(np.float64)
+    return jnp.asarray(np.concatenate([np.cos(wide), np.sin(wide)]).astype(np.float32))
+
+
+def head_scores(hh, cos, sin, q, k_in, qt_s, kt_s, p_s, lam):
+    seq = cos.shape[1]
+    scale = math.log2(math.e) / math.sqrt(DQK)
+    step = 256
+    zero_half = jnp.zeros((DQK, step), BF16)
+    qt = rotate_rows(q, cos, sin).astype(BF16)
+    kt = rotate_rows(k_in, cos, sin).astype(BF16)
+    qt_s[hh] = qt
+    kt_s[hh] = kt
+    k = kt.T
+    for t0 in range(0, seq, step):
+        end = min(t0 + step, seq)
+        tb = end - t0
+        zh = zero_half[:, :tb]
+        q_b = qt[:, t0:end]
+        mask = lax.broadcasted_iota(jnp.int32, (tb, tb), 0) <= lax.broadcasted_iota(jnp.int32, (tb, tb), 1)
+        for m in range(2):
+            half_q = q_b[m * DQK : (m + 1) * DQK]
+            rhs = jnp.concatenate([half_q, zh] if m == 0 else [zh, half_q], axis=0)
+            s = dot(k[:end], rhs)
+            diag = jnp.where(mask, s[t0:], -jnp.inf)
+            s = jnp.concatenate([s[:t0], diag], axis=0) if t0 else diag
+            e = jnp.exp2((s - jnp.max(s, axis=0, keepdims=True)) * scale)
+            r = 1.0 / jnp.sum(e, axis=0, keepdims=True)
+            p_s[hh, m, :end, t0:end] = e * (r if m == 0 else r * -lam)
+
+
+def head_back(hh, cos, sin, lam, qt_s, kt_s, p_s, vt_s, ogt_s, dvt_s, dk_s, bt_s):
+    seq = cos.shape[1]
+    hw = 2 * DQK
+    ve = vt_s.shape[0] // 2
+    inv_root = 1.0 / math.sqrt(DQK)
+    step = 256
+    rows = slice(hh * hw, (hh + 1) * hw)
+    vr = slice(hh * ve, (hh + 1) * ve)
+    qt, kt = qt_s[hh], kt_s[hh]
+    vt = vt_s[vr, :]
+    v = vt.T
+    cb, sb = cos * inv_root, sin * -inv_root
+    for t0 in range(0, seq, step):
+        end = min(t0 + step, seq)
+        q_b = qt[:, t0:end]
+        p1, p2 = p_s[hh, 0, :end, t0:end], p_s[hh, 1, :end, t0:end]
+        mix = (p1 + p2).astype(BF16)
+        ho = dot(vt[:, :end], mix)
+        inv = lax.rsqrt(jnp.mean(ho * ho, axis=0, keepdims=True) + NORM_EPS)
+        og = ogt_s[vr, t0:end].astype(F32)
+        ob = (inv * og - inv * inv * inv * ho * jnp.mean(og * ho, axis=0, keepdims=True)).astype(BF16)
+        mg = dot(v[:end], ob)
+        g1 = (p1 * (mg - jnp.sum(mg * p1, axis=0, keepdims=True))).astype(BF16)
+        g2 = (p2 * (mg + jnp.sum(mg * p2, axis=0, keepdims=True) * (1.0 / lam))).astype(BF16)
+        dvd = dot(ob, mix, 1, 1)
+        dkd = jnp.concatenate([dot(q_b[:DQK], g1, 1, 1), dot(q_b[DQK:], g2, 1, 1)], axis=0)
+        if t0:
+            dvd = jnp.concatenate([dvt_s[vr, :t0] + dvd[:, :t0], dvd[:, t0:]], axis=1)
+            dkd = jnp.concatenate([dk_s[rows, :t0] + dkd[:, :t0], dkd[:, t0:]], axis=1)
+        dvt_s[vr, :end] = dvd
+        dk_s[rows, :end] = dkd
+        dq = jnp.concatenate([dot(kt[:DQK, :end], g1), dot(kt[DQK:, :end], g2)], axis=0)
+        bt_s[rows, t0:end] = rotate_rows(dq, cb[:, t0:end], sb[:, t0:end]).astype(BF16)
+    bt_s[2 * hw + hh * hw : 2 * hw + (hh + 1) * hw, :] = rotate_rows(dk_s[rows, :], cb, sb).astype(BF16)
+
+
+def fused_kernel(sp, dp, pairs, lam_in, rot_in, tok_in, v_in, og_in, wq_in, wk_in,
+                 tg_out, dvr, wg_r,
+                 lam_ref, rot_ref, tok_all, w1, w2, qk_s, vog_src, vog_all, qt_s, kt_s, p_s,
+                 vt_s, ogt_s, dvt_s, dk_s, bt_s, back_m, back_x,
+                 dv_s, sib_s, sib_r, own_s, wz_s, wz_r, tbuf, trecv,
+                 l_s, tok_ss, tok_rs, vog_ss, vog_rs, z_ss, z_rs, s_ss, s_rs, bx_ss, bx_rs, dv_ss, dv_rs,
+                 c_ss, c_rs, g_ss, g_rs, ag_ss, ag_rs, ty_ss, ty_rs):
+    me, mine, z, core, peers, froms, z_to, z_from = places(sp, dp)
+    nz = dp // 2
+    rows, wr = tok_in.shape[0], wq_in.shape[0]
+    half = rows // 2
+    pw = 128
+    sib = (me, mine + 1 - 2 * core)
+    xp, yp = (peers[0], mine), (peers[1], mine)
+
+    def trow(i, start=0, size=rows):
+        return pl.ds(pl.multiple_of(i * rows + start, 16), size)
+
+    def wrow(i):
+        return pl.ds(pl.multiple_of(i * wr, wr), wr)
+
+    def lanes(i, size):
+        return pl.ds(pl.multiple_of(i * size, size), size)
+
+    sends = []
+
+    def go(copy, cond=None):
+        if cond is None:
+            copy.start()
+        else:
+            pl.when(cond)(copy.start)
+        sends.append((copy, cond))
+        return copy
+
+    barrier = pltpu.get_barrier_semaphore()
+    where = [(p, mine) for p in peers] + [(me, zt + core) for zt in z_to] + [sib]
+    for device in where:
+        pl.semaphore_signal(barrier, inc=1, device_id=device, device_id_type=pl.DeviceIdType.MESH)
+
+    count = [0]
+
+    def load(src, dst):
+        c = pltpu.make_async_copy(src, dst, l_s.at[count[0]])
+        count[0] += 1
+        c.start()
+        return c
+
+    def load_weights(w, who):
+        out = []
+        for j in range(pairs):
+            src = lanes(who * pairs + j, pw)
+            out.append(load(wq_in.at[:, src], w.at[wrow(mine), 2 * j * pw : (2 * j + 1) * pw]))
+            out.append(load(wk_in.at[:, src], w.at[wrow(mine), (2 * j + 1) * pw : (2 * j + 2) * pw]))
+        return out
+
+    l_tok = [load(tok_in, tok_all.at[trow(me)])]
+    l_w1 = load_weights(w1, me)
+    l_vog = []
+    for j in range(pairs):
+        for n, src in enumerate((v_in, og_in)):
+            for i, p in enumerate(peers):
+                l_vog.append(load(src.at[:, lanes(p * pairs + j, pw)], vog_src.at[i, j, n]))
+            l_vog.append(load(src.at[:, lanes(me * pairs + j, pw)], vog_all.at[j, n, trow(me)]))
+    l_w2 = load_weights(w2, jnp.where(core == 0, peers[0], peers[1]))
+    l_rot = [load(rot_in, rot_ref), load(lam_in, lam_ref)]
+
+    def z_start(w, k):
+        r = w.at[wrow(mine)]
+        for n, d in enumerate((2, -2, 1, -1)):
+            cond = (z + d < nz) if d > 0 else (z + d >= 0)
+            go(sender(r, r, z_ss.at[k, n], z_rs.at[k, z], (me, (z + d) * 2 + core)), cond)
+        go(sender(r, r, s_ss.at[k, z], s_rs.at[k, z], sib))
+
+    far = lax.rem(z + 2, nz)
+    order = [far, z + 1 - 2 * lax.rem(z, 2), nz - 1 - z]
+
+    def z_step(w, k, i):
+        src = order[i]
+        r = w.at[wrow(2 * src + core)]
+        sender(r, r, z_ss.at[k, 0], z_rs.at[k, src], sib).wait_recv()
+        go(sender(r, r, s_ss.at[k, src], s_rs.at[k, src], sib))
+        if i == 0:
+            inner = jnp.logical_and(z > 0, z < nz - 1)
+            go(sender(r, r, z_ss.at[k, 4], z_rs.at[k, src], (me, (z - 1) * (nz - 1) * 2 + core)), inner)
+
+    def z_sib(w, k):
+        for src in [z] + order:
+            r = w.at[wrow(2 * src + 1 - core)]
+            sender(r, r, s_ss.at[k, 0], s_rs.at[k, src], sib).wait_recv()
+
+    def piece(p, h, k):
+        r = trow(me, h * half, half)
+        return go(sender(tok_all.at[r], tok_all.at[r], tok_ss.at[k], tok_rs.at[k], p))
+
+    for c in l_tok:
+        c.wait()
+    pl.semaphore_wait(barrier, len(where))
+    x0, y1 = piece(xp, 0, 0), piece(yp, 1, 1)
+    x1, y0 = piece(xp, 1, 2), piece(yp, 0, 3)
+    for c in l_w1:
+        c.wait()
+    z_start(w1, 0)
+    for c in l_w2 + l_vog + l_rot:
+        c.wait()
+    x0.wait_recv()
+    f0 = trow(peers[0], 0, half)
+    d0 = go(sender(tok_all.at[f0], tok_all.at[f0], tok_ss.at[4], tok_rs.at[4], yp))
+    y1.wait_recv()
+    f1 = trow(peers[1], half, half)
+    d1 = go(sender(tok_all.at[f1], tok_all.at[f1], tok_ss.at[5], tok_rs.at[5], xp))
+    for j in range(pairs):
+        for i, p in enumerate(peers):
+            go(sender(vog_src.at[i, j], vog_all.at[j, :, trow(me)], vog_ss.at[j, i], vog_rs.at[j, i], (p, mine)))
+    z_step(w1, 0, 0)
+    z_start(w2, 1)
+    z_step(w1, 0, 1)
+    z_step(w1, 0, 2)
+    z_sib(w1, 0)
+    qk_s[trow(me), :] = dot(tok_all[trow(me), :], w1[...])
+    for f, copies in zip(froms, [[x1], [y0], [d0, d1]]):
+        for c in copies:
+            c.wait_recv()
+        qk_s[trow(f), :] = dot(tok_all[trow(f), :], w1[...])
+
+    targets = [lax.rem(z + i, nz) for i in range(1, nz)] + [z]
+    n16 = DQK // 2
+    cos, sin = rot_ref[:n16, :], rot_ref[n16:, :]
+    hw = 2 * DQK
+
+    def one_pair(j):
+        qk = [qk_s[:, (2 * j + n) * pw : (2 * j + n + 1) * pw].T for n in range(2)]
+        lams = [lam_ref[(me * pairs + j) * 2 + hh] for hh in range(2)]
+        for hh in range(2):
+            r = slice(hh * hw, (hh + 1) * hw)
+            head_scores(hh, cos, sin, qk[0][r], qk[1][r], qt_s, kt_s, p_s, lams[hh])
+        for i, p in enumerate(peers):
+            r = vog_all.at[j, :, trow(p)]
+            sender(vog_src.at[i, j], r, vog_ss.at[j, i], vog_rs.at[j, i], (p, mine)).wait_recv()
+        if j == 0:
+            z_step(w2, 1, 0)
+        vt_s[...] = vog_all[j, 0].T
+        ogt_s[...] = vog_all[j, 1].T
+        for hh in range(2):
+            head_back(hh, cos, sin, lams[hh], qt_s, kt_s, p_s, vt_s, ogt_s, dvt_s, dk_s, bt_s)
+        back_m[j] = bt_s[...].T
+        for a, to in enumerate((0, 1)):
+            for b, p in enumerate((peers[to], peers[2])):
+                go(sender(back_m.at[j, trow(p)], back_x.at[a, j, b], bx_ss.at[a, j, b], bx_rs.at[a, j, b], (xp, yp)[to]))
+
+        def weight_part(owner):
+            return dot(bt_s[...], tok_all[:, lanes(owner, wr)])
+
+        for i, zz in enumerate(targets):
+            sib_s[j, i] = weight_part(2 * zz + 1 - core).astype(BF16)
+        for i in range(nz):
+            go(sender(sib_s.at[j, i], sib_r.at[j, i], c_ss.at[j, i], c_rs.at[j, i], sib))
+        for i, zz in enumerate(targets):
+            own_s[j, i] = weight_part(2 * zz + core)
+        dv_s[j] = dvt_s[...].T.astype(BF16)
+        for i, p in enumerate(peers):
+            go(sender(dv_s.at[j, trow(p)], dvr.at[me, j], dv_ss.at[j, i], dv_rs.at[j, i], (p, mine)))
+        dvr[me, j] = dv_s[j, trow(me), :]
+        for i, zz in enumerate(targets):
+            sender(sib_s.at[j, i], sib_r.at[j, i], c_ss.at[j, i], c_rs.at[j, i], sib).wait_recv()
+            part = own_s[j, i] + sib_r[j, i].astype(F32)
+            if i < nz - 1:
+                wz_s[j, i] = part.astype(BF16)
+            else:
+                own_s[j, i] = part
+        for i, zz in enumerate(targets[: nz - 1]):
+            go(sender(wz_s.at[j, i], wz_r.at[j, i], g_ss.at[j, i], g_rs.at[j, i], (me, 2 * zz + core)))
+
+    for j in range(pairs):
+        one_pair(j)
+        if j == 0:
+            z_step(w2, 1, 1)
+    z_step(w2, 1, 2)
+    z_sib(w2, 1)
+
+    def back_wait(a, b):
+        for j in range(pairs):
+            r = back_x.at[a, j, b]
+            sender(r, r, bx_ss.at[a, j, b], bx_rs.at[a, j, b], sib).wait_recv()
+
+    def token_part(who, a, b, c):
+        n = slice((2 * c + a) * wr, (2 * c + a + 1) * wr)
+        out = None
+        for j in range(pairs):
+            k = slice(2 * j * pw, (2 * j + 2) * pw)
+            for lhs, w in ((back_m[j, trow(who), :], w1), (back_x[a, j, b], w2)):
+                part = dot(lhs, w[n, k], 1, 1)
+                out = part if out is None else out + part
+        return out
+
+    ty = []
+    for a in range(2):
+        back_wait(a, 1)
+        for c in range(nz):
+            tbuf[a, c] = token_part(peers[1 - a], a, 1, c).astype(BF16)
+        for c in range(nz):
+            ty.append(go(sender(tbuf.at[a, c], trecv.at[a, c], ty_ss.at[a, c], ty_rs.at[a, c], (yp, xp)[a])))
+
+    def weights_end(j):
+        total = own_s[j, nz - 1]
+        for i in range(nz - 1):
+            r = wz_r.at[j, i]
+            sender(r, r, g_ss.at[j, i], g_rs.at[j, i], sib).wait_recv()
+            total = total + wz_r[j, i].astype(F32)
+        wg_r[me, j] = total.T.astype(BF16)
+        r = wg_r.at[me, j]
+        for i in (2, 0, 1):
+            go(sender(r, r, ag_ss.at[j, i], ag_rs.at[j, i], (peers[i], mine)))
+
+    for j in range(pairs):
+        weights_end(j)
+        if j == 0:
+            for a in range(2):
+                back_wait(a, 0)
+                for c in range(nz):
+                    part = token_part(me, a, 0, c)
+                    ty[a * nz + c].wait_recv()
+                    n = slice((2 * c + a) * wr, (2 * c + a + 1) * wr)
+                    tg_out[:, n] = (part + trecv[a, c].astype(F32)).astype(BF16)
+    for j in range(pairs):
+        for i, p in enumerate(peers):
+            r = dvr.at[p, j]
+            sender(r, r, dv_ss.at[j, i], dv_rs.at[j, i], xp).wait_recv()
+        for i, p in enumerate(peers):
+            r = wg_r.at[p, j]
+            sender(r, r, ag_ss.at[j, i], ag_rs.at[j, i], xp).wait_recv()
+    for c, cond in sends:
+        if cond is None:
+            c.wait_send()
+        else:
+            pl.when(cond)(c.wait_send)
+
+
+def finish_kernel(factor, tg, dvr, wg, tg_out, dv_out, qg_out, kg_out, dv_s, qg, kg, sem):
+    sp, pairs, wr, cols = wg.shape
+    pw = cols // 2
+    copies = [pltpu.make_async_copy(tg, tg_out, sem.at[0])]
+    copies[0].start()
+    for s in range(sp):
+        for j in range(pairs):
+            n = slice((s * pairs + j) * pw, (s * pairs + j + 1) * pw)
+            qg[:, n] = wg[s, j, :, :pw].astype(F32) * factor
+    copies.append(pltpu.make_async_copy(qg, qg_out, sem.at[1]))
+    copies[1].start()
+    for s in range(sp):
+        for j in range(pairs):
+            n = slice((s * pairs + j) * pw, (s * pairs + j + 1) * pw)
+            kg[:, n] = wg[s, j, :, pw:].astype(F32) * factor
+    copies.append(pltpu.make_async_copy(kg, kg_out, sem.at[2]))
+    copies[2].start()
+    for s in range(sp):
+        for j in range(pairs):
+            n = slice((s * pairs + j) * pw, (s * pairs + j + 1) * pw)
+            dv_s[:, n] = dvr[s, j]
+    copies.append(pltpu.make_async_copy(dv_s, dv_out, sem.at[3]))
+    copies[3].start()
+    for c in copies:
+        c.wait()
+
+
+def fused(tok, v, og, wq, wk, lam, rot, sp, dp):
+    rows, width = tok.shape
+    seq = rows * sp
+    wr = wq.shape[0]
+    nz = dp // 2
+    pw = 128
+    pairs = v.shape[1] // (sp * pw)
+    factor = 1.0 / math.sqrt(dp * seq)
+    vm = pl.BlockSpec(memory_space=pltpu.VMEM)
+    anywhere = pl.BlockSpec(memory_space=pl.ANY)
+    dma = pltpu.SemaphoreType.DMA
+    V = pltpu.VMEM
+    tg, dvr, wg = pl.pallas_call(
+        functools.partial(fused_kernel, sp, dp, pairs),
+        out_shape=(
+            V((rows, width), BF16),
+            V((sp, pairs, rows, pw), BF16),
+            V((sp, pairs, wr, 2 * pw), BF16),
+        ),
+        in_specs=[anywhere] * 7,
+        out_specs=(vm,) * 3,
+        scratch_shapes=[
+            pltpu.SMEM(lam.shape, F32), V(rot.shape, F32),
+            V((seq, width), BF16), V((width, 2 * pairs * pw), BF16), V((width, 2 * pairs * pw), BF16),
+            V((seq, 2 * pairs * pw), F32), V((sp - 1, pairs, 2, rows, pw), BF16), V((pairs, 2, seq, pw), BF16),
+            V((2, 2 * DQK, seq), BF16), V((2, 2 * DQK, seq), BF16), V((2, 2, seq, seq), F32),
+            V((pw, seq), BF16), V((pw, seq), BF16), V((pw, seq), F32), V((pw, seq), F32), V((2 * pw, seq), BF16),
+            V((pairs, seq, 2 * pw), BF16), V((2, pairs, 2, rows, 2 * pw), BF16),
+            V((pairs, seq, pw), BF16),
+            V((pairs, nz, 2 * pw, wr), BF16), V((pairs, nz, 2 * pw, wr), BF16), V((pairs, nz, 2 * pw, wr), F32),
+            V((pairs, nz - 1, 2 * pw, wr), BF16), V((pairs, nz - 1, 2 * pw, wr), BF16),
+            V((2, nz, rows, wr), BF16), V((2, nz, rows, wr), BF16),
+            dma((3 + 8 * pairs + 2 * sp * pairs,)),
+            dma((6,)), dma((6,)), dma((pairs, sp - 1)), dma((pairs, sp - 1)),
+            dma((2, 5)), dma((2, nz)), dma((2, nz)), dma((2, nz)),
+            dma((2, pairs, 2)), dma((2, pairs, 2)), dma((pairs, sp - 1)), dma((pairs, sp - 1)),
+            dma((pairs, nz)), dma((pairs, nz)), dma((pairs, nz - 1)), dma((pairs, nz - 1)),
+            dma((pairs, 3)), dma((pairs, 3)), dma((2, nz)), dma((2, nz)),
+        ],
+        compiler_params=pltpu.CompilerParams(
+            vmem_limit_bytes=56 * 1024 * 1024, collective_id=2, has_side_effects=True
+        ),
+        name="fused",
+    )(lam, rot, tok, v, og, wq, wk)
+    return pl.pallas_call(
+        functools.partial(finish_kernel, factor),
+        out_shape=(
+            jax.ShapeDtypeStruct((rows, width), BF16),
+            jax.ShapeDtypeStruct((rows, v.shape[1]), BF16),
+            jax.ShapeDtypeStruct((wr, wq.shape[1]), F32),
+            jax.ShapeDtypeStruct((wr, wq.shape[1]), F32),
+        ),
+        in_specs=[vm] * 3,
+        out_specs=(anywhere,) * 4,
+        scratch_shapes=[V((rows, v.shape[1]), BF16), V((wr, wq.shape[1]), F32), V((wr, wq.shape[1]), F32), dma((4,))],
+        compiler_params=pltpu.CompilerParams(vmem_limit_bytes=16 * 1024 * 1024),
+        name="finish",
+    )(tg, dvr, wg)
+
+
 def body(tokens, query_weight, key_weight, values, lambdas, out_grad):
     sp = lax.axis_size("sp")
     dp = lax.axis_size("dp")
     rows = tokens.shape[1]
     heads = lambdas.shape[0] // sp
+    head_vec = values.shape[2] // lambdas.shape[0]
+    if sp == 4 and dp == 8 and heads % 2 == 0 and head_vec == 64 and rows * sp <= 640:
+        tg, dv, qg, kg = fused(
+            tokens[0], values[0], out_grad[0], query_weight, key_weight, lambdas,
+            position_tables(rows * sp), sp, dp,
+        )
+        return tg[None], dv[None], qg, kg
     cos, sin = rotation_tables(rows * sp)
     tok_all, vog_all, w_all, qk = gather(
         tokens[0], values[0], out_grad[0], query_weight, key_weight, sp, dp

time: 107 us -> 79.2 us (0.74); the launches traced: 105 us -> 79 us
  Pallas kernels: 98.6 us -> 78.2 us
  other arithmetic: 3.75 us -> 0 us
  local copies, waits for them, and re-layouts: 1.57 us -> 0 us
    pallas_call x3 -> x2, Pallas kernels: 98.6 us -> 78.2 us  [the longest x1 76.5 us: fused(): pl.pallas_call(functools.partial(fused_kernel, sp, dp, pairs), out_shape=...]
    mul x1 -> x0, other arithmetic: 2.88 us -> none  [body(): kg.astype(F32) * factor]
    unnamed x6 -> x0, local copies, waits for them, and re-layouts: 1.57 us -> none
where the time goes in v2:
time: 79.2 us; the launch traced here: 79 us
  Pallas kernels  78.2 us (99%)
  between operations  0.8 us (1%)
    pallas_call x1, Pallas kernels, fused(): pl.pallas_call(functools.partial(fused_kernel, sp, dp, pairs), out_shape=...  76.5 us
    pallas_call x1, Pallas kernels, fused(): pl.pallas_call(functools.partial(finish_kernel, factor), out_shape=(jax.S...  1.67 us

profile of v2, /device:TPU:0, one launch (start us, length us, event | category | flops | bytes accessed | tf_op | source)
XLA Modules:
  0.0 79.0 jit_solution(14984062377102229626)
XLA Ops:
  0.6 76.5 %fused.1 = (bf16[160,2048]{1,0:T(8,128)(2,1)S(1)}, bf16[4,2,160,128]{3,2,1,0:T(8,128)(2,1)S(1)}, bf16[4,2,256,256]{3,2,1,0:T(8,128)(2,1)S(1)}) custom-call(f32[16]{0:T(128)} %lam_in.1, f32[32,640]{1,0:T(8,128)} %constant.2.clone.rot_in, bf16[160,2048]{1,0:T(8,128)(2,1)} %bitcast.5, bf16[160,1024]{1,0:T(8,128)(2,1)} %bitcast.6, bf16[160,1024]{1,0:T(8,128)(2,1)} %bitcast.7, ...), custom_call_target="tpu_custom_call" | custom-call | tf_op jit(solution)/shard_map/fused/pallas_call | solution.py:772
  77.2 1.7 %finish.1 = (bf16[160,2048]{1,0:T(8,128)(2,1)}, bf16[160,1024]{1,0:T(8,128)(2,1)}, f32[256,1024]{1,0:T(8,128)}, f32[256,1024]{1,0:T(8,128)}) custom-call(bf16[160,2048]{1,0:T(8,128)(2,1)S(1)} %get-tuple-element.11.tg, bf16[4,2,160,128]{3,2,1,0:T(8,128)(2,1)S(1)} %get-tuple-element.12.dvr, bf16[4,2,256,256]{3,2,1,0:T(8,128)(2,1)S(1)} %get-tuple-element.13.wg), custom_call_target="tpu_custom_call" | custom-call | tf_op jit(solution)/shard_map/finish/pallas_call | solution.py:804

commit v3 on v2

--- a/solution.py
+++ b/solution.py
@@ -457,7 +457,7 @@
             p_s[hh, m, :end, t0:end] = e * (r if m == 0 else r * -lam)
 
 
-def head_back(hh, cos, sin, lam, qt_s, kt_s, p_s, vt_s, ogt_s, dvt_s, dk_s, bt_s):
+def head_back(hh, h, cos, sin, lam, qt_s, kt_s, p_s, vt_s, ogt_s, dvt_s, dk_s, bt_s):
     seq = cos.shape[1]
     hw = 2 * DQK
     ve = vt_s.shape[0] // 2
@@ -465,14 +465,14 @@
     step = 256
     rows = slice(hh * hw, (hh + 1) * hw)
     vr = slice(hh * ve, (hh + 1) * ve)
-    qt, kt = qt_s[hh], kt_s[hh]
+    qt, kt = qt_s[h], kt_s[h]
     vt = vt_s[vr, :]
     v = vt.T
     cb, sb = cos * inv_root, sin * -inv_root
     for t0 in range(0, seq, step):
         end = min(t0 + step, seq)
         q_b = qt[:, t0:end]
-        p1, p2 = p_s[hh, 0, :end, t0:end], p_s[hh, 1, :end, t0:end]
+        p1, p2 = p_s[h, 0, :end, t0:end], p_s[h, 1, :end, t0:end]
         mix = (p1 + p2).astype(BF16)
         ho = dot(vt[:, :end], mix)
         inv = lax.rsqrt(jnp.mean(ho * ho, axis=0, keepdims=True) + NORM_EPS)
@@ -497,9 +497,9 @@
                  tg_out, dvr, wg_r,
                  lam_ref, rot_ref, tok_all, w1, w2, qk_s, vog_src, vog_all, qt_s, kt_s, p_s,
                  vt_s, ogt_s, dvt_s, dk_s, bt_s, back_m, back_x,
-                 dv_s, sib_s, sib_r, own_s, wz_s, wz_r, tbuf, trecv,
+                 dv_s, sib_s, sib_r, own_s, wz_s, wz_r, wz_m, tbuf, trecv, tacc,
                  l_s, tok_ss, tok_rs, vog_ss, vog_rs, z_ss, z_rs, s_ss, s_rs, bx_ss, bx_rs, dv_ss, dv_rs,
-                 c_ss, c_rs, g_ss, g_rs, ag_ss, ag_rs, ty_ss, ty_rs):
+                 c_ss, c_rs, g_ss, g_rs, m_rs, ag_ss, ag_rs, ty_ss, ty_rs):
     me, mine, z, core, peers, froms, z_to, z_from = places(sp, dp)
     nz = dp // 2
     rows, wr = tok_in.shape[0], wq_in.shape[0]
@@ -511,8 +511,8 @@
     def trow(i, start=0, size=rows):
         return pl.ds(pl.multiple_of(i * rows + start, 16), size)
 
-    def wrow(i):
-        return pl.ds(pl.multiple_of(i * wr, wr), wr)
+    def wrow(zz, c):
+        return pl.ds(pl.multiple_of((c * nz + zz) * wr, wr), wr)
 
     def lanes(i, size):
         return pl.ds(pl.multiple_of(i * size, size), size)
@@ -544,11 +544,15 @@
         out = []
         for j in range(pairs):
             src = lanes(who * pairs + j, pw)
-            out.append(load(wq_in.at[:, src], w.at[wrow(mine), 2 * j * pw : (2 * j + 1) * pw]))
-            out.append(load(wk_in.at[:, src], w.at[wrow(mine), (2 * j + 1) * pw : (2 * j + 2) * pw]))
+            out.append(load(wq_in.at[:, src], w.at[wrow(z, core), 2 * j * pw : (2 * j + 1) * pw]))
+            out.append(load(wk_in.at[:, src], w.at[wrow(z, core), (2 * j + 1) * pw : (2 * j + 2) * pw]))
         return out
 
-    l_tok = [load(tok_in, tok_all.at[trow(me)])]
+    l_tok = []
+    for c in range(2):
+        for zz in range(nz):
+            n = slice((c * nz + zz) * wr, (c * nz + zz + 1) * wr)
+            l_tok.append(load(tok_in.at[:, (2 * zz + c) * wr : (2 * zz + c + 1) * wr], tok_all.at[trow(me), n]))
     l_w1 = load_weights(w1, me)
     l_vog = []
     for j in range(pairs):
@@ -559,28 +563,52 @@
     l_w2 = load_weights(w2, jnp.where(core == 0, peers[0], peers[1]))
     l_rot = [load(rot_in, rot_ref), load(lam_in, lam_ref)]
 
-    def z_start(w, k):
-        r = w.at[wrow(mine)]
-        for n, d in enumerate((2, -2, 1, -1)):
-            cond = (z + d < nz) if d > 0 else (z + d >= 0)
-            go(sender(r, r, z_ss.at[k, n], z_rs.at[k, z], (me, (z + d) * 2 + core)), cond)
-        go(sender(r, r, s_ss.at[k, z], s_rs.at[k, z], sib))
-
     far = lax.rem(z + 2, nz)
     order = [far, z + 1 - 2 * lax.rem(z, 2), nz - 1 - z]
-
-    def z_step(w, k, i):
-        src = order[i]
-        r = w.at[wrow(2 * src + core)]
-        sender(r, r, z_ss.at[k, 0], z_rs.at[k, src], sib).wait_recv()
-        go(sender(r, r, s_ss.at[k, src], s_rs.at[k, src], sib))
+    inner = jnp.logical_and(z > 0, z < nz - 1)
+    outer = jnp.logical_not(inner)
+
+    def z_copy(w, k, n, src, to):
+        r = w.at[wrow(src, core)]
+        return sender(r, r, z_ss.at[k, n], z_rs.at[k, src], (me, 2 * to + core))
+
+    def s_copy(w, k, src):
+        r = w.at[wrow(src, core)]
+        return sender(r, r, s_ss.at[k, src], s_rs.at[k, src], sib)
+
+    def z_start():
+        go(z_copy(w1, 0, 0, z, far))
+        go(z_copy(w1, 0, 1, z, order[1]))
+        go(z_copy(w1, 0, 2, z, order[2]), inner)
+        go(s_copy(w1, 0, z))
+
+    def z_step(i):
+        z_copy(w1, 0, 0, order[i], z).wait_recv()
+        go(s_copy(w1, 0, order[i]))
         if i == 0:
-            inner = jnp.logical_and(z > 0, z < nz - 1)
-            go(sender(r, r, z_ss.at[k, 4], z_rs.at[k, src], (me, (z - 1) * (nz - 1) * 2 + core)), inner)
+            go(z_copy(w1, 0, 3, far, order[1]), inner)
+
+    aside = (1 - z // 2) * (nz - 1)
+    near = [order[1], jnp.where(inner, order[2], far)]
+
+    def other_start():
+        go(z_copy(w2, 1, 0, z, far), inner)
+        go(z_copy(w2, 1, 1, z, order[1]))
+        go(z_copy(w2, 1, 2, z, order[2]), inner)
+        go(s_copy(w2, 1, z))
+
+    def other_aside():
+        r = wrow(aside, core)
+        to = (jnp.where(core == 0, peers[0], peers[1]), mine)
+        return sender(w1.at[r], w2.at[r], z_ss.at[1, 3], z_rs.at[1, aside], to)
+
+    def other_step(src):
+        z_copy(w2, 1, 0, src, z).wait_recv()
+        go(s_copy(w2, 1, src))
 
     def z_sib(w, k):
         for src in [z] + order:
-            r = w.at[wrow(2 * src + 1 - core)]
+            r = w.at[wrow(src, 1 - core)]
             sender(r, r, s_ss.at[k, 0], s_rs.at[k, src], sib).wait_recv()
 
     def piece(p, h, k):
@@ -594,7 +622,7 @@
     x1, y0 = piece(xp, 1, 2), piece(yp, 0, 3)
     for c in l_w1:
         c.wait()
-    z_start(w1, 0)
+    z_start()
     for c in l_w2 + l_vog + l_rot:
         c.wait()
     x0.wait_recv()
@@ -603,13 +631,17 @@
     y1.wait_recv()
     f1 = trow(peers[1], half, half)
     d1 = go(sender(tok_all.at[f1], tok_all.at[f1], tok_ss.at[5], tok_rs.at[5], xp))
-    for j in range(pairs):
-        for i, p in enumerate(peers):
-            go(sender(vog_src.at[i, j], vog_all.at[j, :, trow(me)], vog_ss.at[j, i], vog_rs.at[j, i], (p, mine)))
-    z_step(w1, 0, 0)
-    z_start(w2, 1)
-    z_step(w1, 0, 1)
-    z_step(w1, 0, 2)
+
+    def vog_start(j):
+        for i in range(sp - 1):
+            dst = vog_all.at[j, :, trow(me)]
+            go(sender(vog_src.at[i, j], dst, vog_ss.at[j, i], vog_rs.at[j, i], (peers[i], mine)))
+
+    vog_start(0)
+    z_step(0)
+    other_start()
+    z_step(1)
+    z_step(2)
     z_sib(w1, 0)
     qk_s[trow(me), :] = dot(tok_all[trow(me), :], w1[...])
     for f, copies in zip(froms, [[x1], [y0], [d0, d1]]):
@@ -617,112 +649,166 @@
             c.wait_recv()
         qk_s[trow(f), :] = dot(tok_all[trow(f), :], w1[...])
 
-    targets = [lax.rem(z + i, nz) for i in range(1, nz)] + [z]
     n16 = DQK // 2
     cos, sin = rot_ref[:n16, :], rot_ref[n16:, :]
     hw = 2 * DQK
 
-    def one_pair(j):
+    lams = [lam_ref[me * pairs * 2 + h] for h in range(2 * pairs)]
+    def scores(j):
         qk = [qk_s[:, (2 * j + n) * pw : (2 * j + n + 1) * pw].T for n in range(2)]
-        lams = [lam_ref[(me * pairs + j) * 2 + hh] for hh in range(2)]
         for hh in range(2):
             r = slice(hh * hw, (hh + 1) * hw)
-            head_scores(hh, cos, sin, qk[0][r], qk[1][r], qt_s, kt_s, p_s, lams[hh])
+            h = 2 * j + hh
+            head_scores(h, cos, sin, qk[0][r], qk[1][r], qt_s, kt_s, p_s, lams[h])
+
+    def values_start(j):
+        for i, p in enumerate(peers):
+            go(sender(dv_s.at[j, trow(p)], dvr.at[me, j], dv_ss.at[j, i], dv_rs.at[j, i], (p, mine)))
+        dvr[me, j] = dv_s[j, trow(me), :]
+
+    def one_pair(j):
         for i, p in enumerate(peers):
             r = vog_all.at[j, :, trow(p)]
             sender(vog_src.at[i, j], r, vog_ss.at[j, i], vog_rs.at[j, i], (p, mine)).wait_recv()
         if j == 0:
-            z_step(w2, 1, 0)
+            go(other_aside())
         vt_s[...] = vog_all[j, 0].T
         ogt_s[...] = vog_all[j, 1].T
         for hh in range(2):
-            head_back(hh, cos, sin, lams[hh], qt_s, kt_s, p_s, vt_s, ogt_s, dvt_s, dk_s, bt_s)
+            head_back(hh, 2 * j + hh, cos, sin, lams[2 * j + hh], qt_s, kt_s, p_s, vt_s, ogt_s, dvt_s, dk_s, bt_s)
         back_m[j] = bt_s[...].T
         for a, to in enumerate((0, 1)):
             for b, p in enumerate((peers[to], peers[2])):
                 go(sender(back_m.at[j, trow(p)], back_x.at[a, j, b], bx_ss.at[a, j, b], bx_rs.at[a, j, b], (xp, yp)[to]))
 
-        def weight_part(owner):
-            return dot(bt_s[...], tok_all[:, lanes(owner, wr)])
-
-        for i, zz in enumerate(targets):
-            sib_s[j, i] = weight_part(2 * zz + 1 - core).astype(BF16)
+        def weight_part(c):
+            return dot(bt_s[...], tok_all[:, lanes(c, nz * wr)])
+
+        part = weight_part(1 - core)
+        for zz in range(nz):
+            sib_s[j, zz] = part[:, zz * wr : (zz + 1) * wr].astype(BF16)
+        for zz in range(nz):
+            go(sender(sib_s.at[j, zz], sib_r.at[j, zz], c_ss.at[j, zz], c_rs.at[j, zz], sib))
+        part = weight_part(core)
+        for zz in range(nz):
+            own_s[j, zz] = part[:, zz * wr : (zz + 1) * wr]
+        dv_s[j] = dvt_s[...].T.astype(BF16)
+        values_start(j)
+        if j:
+            merge(j - 1)
         for i in range(nz):
-            go(sender(sib_s.at[j, i], sib_r.at[j, i], c_ss.at[j, i], c_rs.at[j, i], sib))
-        for i, zz in enumerate(targets):
-            own_s[j, i] = weight_part(2 * zz + core)
-        dv_s[j] = dvt_s[...].T.astype(BF16)
-        for i, p in enumerate(peers):
-            go(sender(dv_s.at[j, trow(p)], dvr.at[me, j], dv_ss.at[j, i], dv_rs.at[j, i], (p, mine)))
-        dvr[me, j] = dv_s[j, trow(me), :]
-        for i, zz in enumerate(targets):
             sender(sib_s.at[j, i], sib_r.at[j, i], c_ss.at[j, i], c_rs.at[j, i], sib).wait_recv()
-            part = own_s[j, i] + sib_r[j, i].astype(F32)
-            if i < nz - 1:
-                wz_s[j, i] = part.astype(BF16)
-            else:
-                own_s[j, i] = part
-        for i, zz in enumerate(targets[: nz - 1]):
-            go(sender(wz_s.at[j, i], wz_r.at[j, i], g_ss.at[j, i], g_rs.at[j, i], (me, 2 * zz + core)))
+            own_s[j, i] = own_s[j, i] + sib_r[j, i].astype(F32)
+        for i in range(nz - 1):
+            wz_s[j, i] = own_s[j, order[i]].astype(BF16)
+        go(sender(wz_s.at[j, 2], wz_m.at[j], g_ss.at[j, 2], m_rs.at[j], (me, 2 * order[1] + core)), outer)
+        go(z_share(j, 0), outer)
+        go(z_share(j, 2), inner)
+        go(z_share(j, 1))
+
+    def z_share(j, i):
+        return sender(wz_s.at[j, i], wz_r.at[j, i], g_ss.at[j, i], g_rs.at[j, i], (me, 2 * order[i] + core))
+
+    def merge(j):
+        c = z_share(j, 0)
+
+        @pl.when(inner)
+        def _():
+            sender(wz_m.at[j], wz_m.at[j], g_ss.at[j, 0], m_rs.at[j], sib).wait_recv()
+            wz_s[j, 0] = (own_s[j, far] + wz_m[j].astype(F32)).astype(BF16)
+            c.start()
+
+        sends.append((c, inner))
 
     for j in range(pairs):
+        scores(j)
+        if j == 0:
+            for jj in range(1, pairs):
+                vog_start(jj)
         one_pair(j)
         if j == 0:
-            z_step(w2, 1, 1)
-    z_step(w2, 1, 2)
+            other_step(near[0])
+
+    def back_wait(a, j, b):
+        r = back_x.at[a, j, b]
+        sender(r, r, bx_ss.at[a, j, b], bx_rs.at[a, j, b], sib).wait_recv()
+
+    def token_part(who, a, b, parts):
+        n = slice(a * nz * wr, (a + 1) * nz * wr)
+        out = None
+        for j, own in parts:
+            k = slice(2 * j * pw, (2 * j + 2) * pw)
+            part = dot(back_m[j, trow(who), :], w1[n, k], 1, 1) if own else dot(back_x[a, j, b], w2[n, k], 1, 1)
+            out = part if out is None else out + part
+        return out
+
+    early = [(j, True) for j in range(pairs)] + [(j, False) for j in range(pairs - 1)]
+    late = [(pairs - 1, False)]
+    other_step(near[1])
+    other_step(aside)
     z_sib(w2, 1)
-
-    def back_wait(a, b):
-        for j in range(pairs):
-            r = back_x.at[a, j, b]
-            sender(r, r, bx_ss.at[a, j, b], bx_rs.at[a, j, b], sib).wait_recv()
-
-    def token_part(who, a, b, c):
-        n = slice((2 * c + a) * wr, (2 * c + a + 1) * wr)
-        out = None
-        for j in range(pairs):
-            k = slice(2 * j * pw, (2 * j + 2) * pw)
-            for lhs, w in ((back_m[j, trow(who), :], w1), (back_x[a, j, b], w2)):
-                part = dot(lhs, w[n, k], 1, 1)
-                out = part if out is None else out + part
-        return out
-
-    ty = []
     for a in range(2):
-        back_wait(a, 1)
-        for c in range(nz):
-            tbuf[a, c] = token_part(peers[1 - a], a, 1, c).astype(BF16)
-        for c in range(nz):
-            ty.append(go(sender(tbuf.at[a, c], trecv.at[a, c], ty_ss.at[a, c], ty_rs.at[a, c], (yp, xp)[a])))
+        for b in range(2):
+            for j in range(pairs - 1):
+                back_wait(a, j, b)
+    for a in range(2):
+        tacc[a] = token_part(peers[1 - a], a, 1, early)
+    ty = {}
+    for a in range(2):
+        back_wait(a, pairs - 1, 1)
+        tbuf[a] = (tacc[a] + token_part(peers[1 - a], a, 1, late)).astype(BF16)
+        for h in range(2):
+            r = pl.ds(h * half, half)
+            ty[a, h] = go(sender(tbuf.at[a, r], trecv.at[a, r], ty_ss.at[a, h], ty_rs.at[a, h], (yp, xp)[a]))
 
     def weights_end(j):
-        total = own_s[j, nz - 1]
-        for i in range(nz - 1):
-            r = wz_r.at[j, i]
-            sender(r, r, g_ss.at[j, i], g_rs.at[j, i], sib).wait_recv()
-            total = total + wz_r[j, i].astype(F32)
+        @pl.when(inner)
+        def _():
+            z_share(j, 2).wait_recv()
+            own_s[j, z] = own_s[j, z] + wz_r[j, 2].astype(F32)
+
+        z_share(j, 0).wait_recv()
+        z_share(j, 1).wait_recv()
+        total = own_s[j, z] + wz_r[j, 0].astype(F32) + wz_r[j, 1].astype(F32)
         wg_r[me, j] = total.T.astype(BF16)
-        r = wg_r.at[me, j]
-        for i in (2, 0, 1):
-            go(sender(r, r, ag_ss.at[j, i], ag_rs.at[j, i], (peers[i], mine)))
-
+        for h, k, to in ((0, 0, xp), (1, 1, yp), (1, 2, xp), (0, 3, yp)):
+            go(ag(me, j, h, k, to))
+
+    wh = wr // 2
+
+    def ag(owner, j, h, k, to):
+        r = wg_r.at[owner, j, pl.ds(h * wh, wh)]
+        return sender(r, r, ag_ss.at[j, k], ag_rs.at[j, k], to)
+
+    def weights_relay(j):
+        ag(peers[0], j, 0, 0, xp).wait_recv()
+        go(ag(peers[0], j, 0, 4, yp))
+        ag(peers[1], j, 1, 1, yp).wait_recv()
+        go(ag(peers[1], j, 1, 5, xp))
+
+    merge(pairs - 1)
+    weights_end(0)
+    for a in range(2):
+        back_wait(a, pairs - 1, 0)
+    for a in range(2):
+        tacc[a] = token_part(me, a, 0, early + late)
+    for j in range(1, pairs):
+        weights_end(j)
+    for h in range(2):
+        for a in range(2):
+            ty[a, h].wait_recv()
+            r = slice(h * half, (h + 1) * half)
+            total = (tacc[a, r] + trecv[a, r].astype(F32)).astype(BF16)
+            for zz in range(nz):
+                tg_out[r, (2 * zz + a) * wr : (2 * zz + a + 1) * wr] = total[:, zz * wr : (zz + 1) * wr]
     for j in range(pairs):
-        weights_end(j)
-        if j == 0:
-            for a in range(2):
-                back_wait(a, 0)
-                for c in range(nz):
-                    part = token_part(me, a, 0, c)
-                    ty[a * nz + c].wait_recv()
-                    n = slice((2 * c + a) * wr, (2 * c + a + 1) * wr)
-                    tg_out[:, n] = (part + trecv[a, c].astype(F32)).astype(BF16)
+        weights_relay(j)
     for j in range(pairs):
         for i, p in enumerate(peers):
             r = dvr.at[p, j]
             sender(r, r, dv_ss.at[j, i], dv_rs.at[j, i], xp).wait_recv()
-        for i, p in enumerate(peers):
-            r = wg_r.at[p, j]
-            sender(r, r, ag_ss.at[j, i], ag_rs.at[j, i], xp).wait_recv()
+        for owner, h, k in ((peers[0], 1, 2), (peers[1], 0, 3), (peers[2], 0, 4), (peers[2], 1, 5)):
+            ag(owner, j, h, k, xp).wait_recv()
     for c, cond in sends:
         if cond is None:
             c.wait_send()
@@ -782,19 +868,19 @@
             pltpu.SMEM(lam.shape, F32), V(rot.shape, F32),
             V((seq, width), BF16), V((width, 2 * pairs * pw), BF16), V((width, 2 * pairs * pw), BF16),
             V((seq, 2 * pairs * pw), F32), V((sp - 1, pairs, 2, rows, pw), BF16), V((pairs, 2, seq, pw), BF16),
-            V((2, 2 * DQK, seq), BF16), V((2, 2 * DQK, seq), BF16), V((2, 2, seq, seq), F32),
+            V((2 * pairs, 2 * DQK, seq), BF16), V((2 * pairs, 2 * DQK, seq), BF16), V((2 * pairs, 2, seq, seq), F32),
             V((pw, seq), BF16), V((pw, seq), BF16), V((pw, seq), F32), V((pw, seq), F32), V((2 * pw, seq), BF16),
             V((pairs, seq, 2 * pw), BF16), V((2, pairs, 2, rows, 2 * pw), BF16),
             V((pairs, seq, pw), BF16),
             V((pairs, nz, 2 * pw, wr), BF16), V((pairs, nz, 2 * pw, wr), BF16), V((pairs, nz, 2 * pw, wr), F32),
-            V((pairs, nz - 1, 2 * pw, wr), BF16), V((pairs, nz - 1, 2 * pw, wr), BF16),
-            V((2, nz, rows, wr), BF16), V((2, nz, rows, wr), BF16),
-            dma((3 + 8 * pairs + 2 * sp * pairs,)),
+            V((pairs, nz - 1, 2 * pw, wr), BF16), V((pairs, nz - 1, 2 * pw, wr), BF16), V((pairs, 2 * pw, wr), BF16),
+            V((2, rows, nz * wr), BF16), V((2, rows, nz * wr), BF16), V((2, rows, nz * wr), F32),
+            dma((2 + dp + 8 * pairs + 2 * sp * pairs,)),
             dma((6,)), dma((6,)), dma((pairs, sp - 1)), dma((pairs, sp - 1)),
-            dma((2, 5)), dma((2, nz)), dma((2, nz)), dma((2, nz)),
+            dma((2, 4)), dma((2, nz)), dma((2, nz)), dma((2, nz)),
             dma((2, pairs, 2)), dma((2, pairs, 2)), dma((pairs, sp - 1)), dma((pairs, sp - 1)),
-            dma((pairs, nz)), dma((pairs, nz)), dma((pairs, nz - 1)), dma((pairs, nz - 1)),
-            dma((pairs, 3)), dma((pairs, 3)), dma((2, nz)), dma((2, nz)),
+            dma((pairs, nz)), dma((pairs, nz)), dma((pairs, nz - 1)), dma((pairs, nz - 1)), dma((pairs,)),
+            dma((pairs, 6)), dma((pairs, 6)), dma((2, 2)), dma((2, 2)),
         ],
         compiler_params=pltpu.CompilerParams(
             vmem_limit_bytes=56 * 1024 * 1024, collective_id=2, has_side_effects=True

time: 79.2 us -> 72.8 us (0.919)
  Pallas kernels: 78.2 us -> 71.9 us
    pallas_call x1, Pallas kernels: 76.5 us -> 70.2 us  [fused(): pl.pallas_call(functools.partial(fused_kernel, sp, dp, pairs), out_shape=...]
where the time goes in v3:
time: 72.8 us; the launch traced here: 72.7 us
  Pallas kernels  71.9 us (99%)
  between operations  0.8 us (1%)
    pallas_call x1, Pallas kernels, fused(): pl.pallas_call(functools.partial(fused_kernel, sp, dp, pairs), out_shape=...  70.2 us
    pallas_call x1, Pallas kernels, fused(): pl.pallas_call(functools.partial(finish_kernel, factor), out_shape=(jax.S...  1.67 us

profile of v3, /device:TPU:0, one launch (start us, length us, event | category | flops | bytes accessed | tf_op | source)
XLA Modules:
  0.0 72.7 jit_solution(15680809869550212962)
XLA Ops:
  0.6 70.2 %fused.1 = (bf16[160,2048]{1,0:T(8,128)(2,1)S(1)}, bf16[4,2,160,128]{3,2,1,0:T(8,128)(2,1)S(1)}, bf16[4,2,256,256]{3,2,1,0:T(8,128)(2,1)S(1)}) custom-call(f32[16]{0:T(128)} %lam_in.1, f32[32,640]{1,0:T(8,128)} %constant.2.clone.rot_in, bf16[160,2048]{1,0:T(8,128)(2,1)} %bitcast.5, bf16[160,1024]{1,0:T(8,128)(2,1)} %bitcast.6, bf16[160,1024]{1,0:T(8,128)(2,1)} %bitcast.7, ...), custom_call_target="tpu_custom_call" | custom-call | tf_op jit(solution)/shard_map/fused/pallas_call | solution.py:858
  70.8 1.7 %finish.1 = (bf16[160,2048]{1,0:T(8,128)(2,1)}, bf16[160,1024]{1,0:T(8,128)(2,1)}, f32[256,1024]{1,0:T(8,128)}, f32[256,1024]{1,0:T(8,128)}) custom-call(bf16[160,2048]{1,0:T(8,128)(2,1)S(1)} %get-tuple-element.11.tg, bf16[4,2,160,128]{3,2,1,0:T(8,128)(2,1)S(1)} %get-tuple-element.12.dvr, bf16[4,2,256,256]{3,2,1,0:T(8,128)(2,1)S(1)} %get-tuple-element.13.wg), custom_call_target="tpu_custom_call" | custom-call | tf_op jit(solution)/shard_map/finish/pallas_call | solution.py:890

commit v4 on v3

--- a/solution.py
+++ b/solution.py
@@ -457,40 +457,47 @@
             p_s[hh, m, :end, t0:end] = e * (r if m == 0 else r * -lam)
 
 
-def head_back(hh, h, cos, sin, lam, qt_s, kt_s, p_s, vt_s, ogt_s, dvt_s, dk_s, bt_s):
+def pair_back(h0, cos, sin, lams, qt_s, kt_s, p_s, vt_s, ogt_s, dvt_s, dk_s, bt_s):
     seq = cos.shape[1]
     hw = 2 * DQK
     ve = vt_s.shape[0] // 2
     inv_root = 1.0 / math.sqrt(DQK)
     step = 256
-    rows = slice(hh * hw, (hh + 1) * hw)
-    vr = slice(hh * ve, (hh + 1) * ve)
-    qt, kt = qt_s[h], kt_s[h]
-    vt = vt_s[vr, :]
-    v = vt.T
     cb, sb = cos * inv_root, sin * -inv_root
-    for t0 in range(0, seq, step):
-        end = min(t0 + step, seq)
-        q_b = qt[:, t0:end]
-        p1, p2 = p_s[h, 0, :end, t0:end], p_s[h, 1, :end, t0:end]
-        mix = (p1 + p2).astype(BF16)
-        ho = dot(vt[:, :end], mix)
-        inv = lax.rsqrt(jnp.mean(ho * ho, axis=0, keepdims=True) + NORM_EPS)
-        og = ogt_s[vr, t0:end].astype(F32)
-        ob = (inv * og - inv * inv * inv * ho * jnp.mean(og * ho, axis=0, keepdims=True)).astype(BF16)
-        mg = dot(v[:end], ob)
-        g1 = (p1 * (mg - jnp.sum(mg * p1, axis=0, keepdims=True))).astype(BF16)
-        g2 = (p2 * (mg + jnp.sum(mg * p2, axis=0, keepdims=True) * (1.0 / lam))).astype(BF16)
-        dvd = dot(ob, mix, 1, 1)
-        dkd = jnp.concatenate([dot(q_b[:DQK], g1, 1, 1), dot(q_b[DQK:], g2, 1, 1)], axis=0)
+    work = [(hh, t0, min(t0 + step, seq)) for t0 in range(0, seq, step) for hh in range(2)]
+    rows = [slice(hh * hw, (hh + 1) * hw) for hh in range(2)]
+    vrows = [slice(hh * ve, (hh + 1) * ve) for hh in range(2)]
+    vt = [vt_s[r, :] for r in vrows]
+    v = [x.T for x in vt]
+    mix, ho, ob, g1, g2 = {}, {}, {}, {}, {}
+    for w in work:
+        hh, t0, end = w
+        mix[w] = (p_s[h0 + hh, 0, :end, t0:end] + p_s[h0 + hh, 1, :end, t0:end]).astype(BF16)
+        ho[w] = dot(vt[hh][:, :end], mix[w])
+    for w in work:
+        hh, t0, end = w
+        x = ho[w]
+        inv = lax.rsqrt(jnp.mean(x * x, axis=0, keepdims=True) + NORM_EPS)
+        og = ogt_s[vrows[hh], t0:end].astype(F32)
+        ob[w] = (inv * og - inv * inv * inv * x * jnp.mean(og * x, axis=0, keepdims=True)).astype(BF16)
+    for w in work:
+        hh, t0, end = w
+        mg = dot(v[hh][:end], ob[w])
+        p1, p2 = p_s[h0 + hh, 0, :end, t0:end], p_s[h0 + hh, 1, :end, t0:end]
+        g1[w] = (p1 * (mg - jnp.sum(mg * p1, axis=0, keepdims=True))).astype(BF16)
+        g2[w] = (p2 * (mg + jnp.sum(mg * p2, axis=0, keepdims=True) * (1.0 / lams[hh]))).astype(BF16)
+        q_b, kt = qt_s[h0 + hh, :, t0:end], kt_s[h0 + hh]
+        dq = jnp.concatenate([dot(kt[:DQK, :end], g1[w]), dot(kt[DQK:, :end], g2[w])], axis=0)
+        bt_s[rows[hh], t0:end] = rotate_rows(dq, cb[:, t0:end], sb[:, t0:end]).astype(BF16)
+        dvd = dot(ob[w], mix[w], 1, 1)
+        dkd = jnp.concatenate([dot(q_b[:DQK], g1[w], 1, 1), dot(q_b[DQK:], g2[w], 1, 1)], axis=0)
         if t0:
-            dvd = jnp.concatenate([dvt_s[vr, :t0] + dvd[:, :t0], dvd[:, t0:]], axis=1)
-            dkd = jnp.concatenate([dk_s[rows, :t0] + dkd[:, :t0], dkd[:, t0:]], axis=1)
-        dvt_s[vr, :end] = dvd
-        dk_s[rows, :end] = dkd
-        dq = jnp.concatenate([dot(kt[:DQK, :end], g1), dot(kt[DQK:, :end], g2)], axis=0)
-        bt_s[rows, t0:end] = rotate_rows(dq, cb[:, t0:end], sb[:, t0:end]).astype(BF16)
-    bt_s[2 * hw + hh * hw : 2 * hw + (hh + 1) * hw, :] = rotate_rows(dk_s[rows, :], cb, sb).astype(BF16)
+            dvd = jnp.concatenate([dvt_s[vrows[hh], :t0] + dvd[:, :t0], dvd[:, t0:]], axis=1)
+            dkd = jnp.concatenate([dk_s[rows[hh], :t0] + dkd[:, :t0], dkd[:, t0:]], axis=1)
+        dvt_s[vrows[hh], :end] = dvd
+        dk_s[rows[hh], :end] = dkd
+    for hh in range(2):
+        bt_s[2 * hw + hh * hw : 2 * hw + (hh + 1) * hw, :] = rotate_rows(dk_s[rows[hh], :], cb, sb).astype(BF16)
 
 
 def fused_kernel(sp, dp, pairs, lam_in, rot_in, tok_in, v_in, og_in, wq_in, wk_in,
@@ -498,8 +505,7 @@
                  lam_ref, rot_ref, tok_all, w1, w2, qk_s, vog_src, vog_all, qt_s, kt_s, p_s,
                  vt_s, ogt_s, dvt_s, dk_s, bt_s, back_m, back_x,
                  dv_s, sib_s, sib_r, own_s, wz_s, wz_r, wz_m, tbuf, trecv, tacc,
-                 l_s, tok_ss, tok_rs, vog_ss, vog_rs, z_ss, z_rs, s_ss, s_rs, bx_ss, bx_rs, dv_ss, dv_rs,
-                 c_ss, c_rs, g_ss, g_rs, m_rs, ag_ss, ag_rs, ty_ss, ty_rs):
+                 pool, tok_rs, vog_rs, z_rs, s_rs, bx_rs, dv_rs, c_rs, g_rs, m_rs, ag_rs, ty_rs):
     me, mine, z, core, peers, froms, z_to, z_from = places(sp, dp)
     nz = dp // 2
     rows, wr = tok_in.shape[0], wq_in.shape[0]
@@ -518,27 +524,52 @@
         return pl.ds(pl.multiple_of(i * size, size), size)
 
     sends = []
-
-    def go(copy, cond=None):
+    free = list(range(pool.shape[0]))
+
+    def remote(src, dst, rsem, device):
+        return lambda ssem: sender(src, dst, ssem, rsem, device)
+
+    def arrive(link):
+        link(pool.at[0]).wait_recv()
+
+    def ready(link, cond=None):
+        slot = free.pop(0)
+        copy = link(pool.at[slot])
+        sends.append((copy, cond, slot))
+        return copy
+
+    def go(link, cond=None):
+        copy = ready(link, cond)
         if cond is None:
             copy.start()
         else:
             pl.when(cond)(copy.start)
-        sends.append((copy, cond))
-        return copy
+        return link
+
+    def flush(count):
+        for c, cond, slot in sends[:count]:
+            if cond is None:
+                c.wait_send()
+            else:
+                pl.when(cond)(c.wait_send)
+            free.append(slot)
+        del sends[:count]
 
     barrier = pltpu.get_barrier_semaphore()
     where = [(p, mine) for p in peers] + [(me, zt + core) for zt in z_to] + [sib]
     for device in where:
         pl.semaphore_signal(barrier, inc=1, device_id=device, device_id_type=pl.DeviceIdType.MESH)
 
-    count = [0]
-
     def load(src, dst):
-        c = pltpu.make_async_copy(src, dst, l_s.at[count[0]])
-        count[0] += 1
+        slot = free.pop(0)
+        c = pltpu.make_async_copy(src, dst, pool.at[slot])
         c.start()
-        return c
+        return c, slot
+
+    def loaded(copies):
+        for c, slot in copies:
+            c.wait()
+            free.append(slot)
 
     def load_weights(w, who):
         out = []
@@ -554,15 +585,6 @@
             n = slice((c * nz + zz) * wr, (c * nz + zz + 1) * wr)
             l_tok.append(load(tok_in.at[:, (2 * zz + c) * wr : (2 * zz + c + 1) * wr], tok_all.at[trow(me), n]))
     l_w1 = load_weights(w1, me)
-    l_vog = []
-    for j in range(pairs):
-        for n, src in enumerate((v_in, og_in)):
-            for i, p in enumerate(peers):
-                l_vog.append(load(src.at[:, lanes(p * pairs + j, pw)], vog_src.at[i, j, n]))
-            l_vog.append(load(src.at[:, lanes(me * pairs + j, pw)], vog_all.at[j, n, trow(me)]))
-    l_w2 = load_weights(w2, jnp.where(core == 0, peers[0], peers[1]))
-    l_rot = [load(rot_in, rot_ref), load(lam_in, lam_ref)]
-
     far = lax.rem(z + 2, nz)
     order = [far, z + 1 - 2 * lax.rem(z, 2), nz - 1 - z]
     inner = jnp.logical_and(z > 0, z < nz - 1)
@@ -570,11 +592,11 @@
 
     def z_copy(w, k, n, src, to):
         r = w.at[wrow(src, core)]
-        return sender(r, r, z_ss.at[k, n], z_rs.at[k, src], (me, 2 * to + core))
+        return remote(r, r, z_rs.at[k, src], (me, 2 * to + core))
 
     def s_copy(w, k, src):
         r = w.at[wrow(src, core)]
-        return sender(r, r, s_ss.at[k, src], s_rs.at[k, src], sib)
+        return remote(r, r, s_rs.at[k, src], sib)
 
     def z_start():
         go(z_copy(w1, 0, 0, z, far))
@@ -583,7 +605,7 @@
         go(s_copy(w1, 0, z))
 
     def z_step(i):
-        z_copy(w1, 0, 0, order[i], z).wait_recv()
+        arrive(z_copy(w1, 0, 0, order[i], z))
         go(s_copy(w1, 0, order[i]))
         if i == 0:
             go(z_copy(w1, 0, 3, far, order[1]), inner)
@@ -600,53 +622,58 @@
     def other_aside():
         r = wrow(aside, core)
         to = (jnp.where(core == 0, peers[0], peers[1]), mine)
-        return sender(w1.at[r], w2.at[r], z_ss.at[1, 3], z_rs.at[1, aside], to)
+        return remote(w1.at[r], w2.at[r], z_rs.at[1, aside], to)
 
     def other_step(src):
-        z_copy(w2, 1, 0, src, z).wait_recv()
+        arrive(z_copy(w2, 1, 0, src, z))
         go(s_copy(w2, 1, src))
 
     def z_sib(w, k):
         for src in [z] + order:
             r = w.at[wrow(src, 1 - core)]
-            sender(r, r, s_ss.at[k, 0], s_rs.at[k, src], sib).wait_recv()
+            arrive(remote(r, r, s_rs.at[k, src], sib))
 
     def piece(p, h, k):
         r = trow(me, h * half, half)
-        return go(sender(tok_all.at[r], tok_all.at[r], tok_ss.at[k], tok_rs.at[k], p))
-
-    for c in l_tok:
-        c.wait()
+        return go(remote(tok_all.at[r], tok_all.at[r], tok_rs.at[k], p))
+
+    loaded(l_tok)
     pl.semaphore_wait(barrier, len(where))
     x0, y1 = piece(xp, 0, 0), piece(yp, 1, 1)
     x1, y0 = piece(xp, 1, 2), piece(yp, 0, 3)
-    for c in l_w1:
-        c.wait()
+    loaded(l_w1)
     z_start()
-    for c in l_w2 + l_vog + l_rot:
-        c.wait()
-    x0.wait_recv()
+    l_vog = []
+    for n, src in enumerate((v_in, og_in)):
+        for i, p in enumerate(peers):
+            l_vog.append(load(src.at[:, lanes(p, pairs * pw)], vog_src.at[i, n]))
+        l_vog.append(load(src.at[:, lanes(me, pairs * pw)], vog_all.at[n, trow(me)]))
+    l_w2 = load_weights(w2, jnp.where(core == 0, peers[0], peers[1]))
+    l_rot = [load(rot_in, rot_ref), load(lam_in, lam_ref)]
+    loaded(l_w2 + l_vog + l_rot)
+    arrive(x0)
     f0 = trow(peers[0], 0, half)
-    d0 = go(sender(tok_all.at[f0], tok_all.at[f0], tok_ss.at[4], tok_rs.at[4], yp))
-    y1.wait_recv()
+    d0 = go(remote(tok_all.at[f0], tok_all.at[f0], tok_rs.at[4], yp))
+    arrive(y1)
     f1 = trow(peers[1], half, half)
-    d1 = go(sender(tok_all.at[f1], tok_all.at[f1], tok_ss.at[5], tok_rs.at[5], xp))
+    d1 = go(remote(tok_all.at[f1], tok_all.at[f1], tok_rs.at[5], xp))
 
     def vog_start(j):
         for i in range(sp - 1):
-            dst = vog_all.at[j, :, trow(me)]
-            go(sender(vog_src.at[i, j], dst, vog_ss.at[j, i], vog_rs.at[j, i], (peers[i], mine)))
+            n = slice(j * pw, (j + 1) * pw)
+            dst = vog_all.at[:, trow(me), n]
+            go(remote(vog_src.at[i, :, :, n], dst, vog_rs.at[j, i], (peers[i], mine)))
 
     vog_start(0)
     z_step(0)
-    other_start()
     z_step(1)
     z_step(2)
+    other_start()
     z_sib(w1, 0)
     qk_s[trow(me), :] = dot(tok_all[trow(me), :], w1[...])
     for f, copies in zip(froms, [[x1], [y0], [d0, d1]]):
         for c in copies:
-            c.wait_recv()
+            arrive(c)
         qk_s[trow(f), :] = dot(tok_all[trow(f), :], w1[...])
 
     n16 = DQK // 2
@@ -663,23 +690,25 @@
 
     def values_start(j):
         for i, p in enumerate(peers):
-            go(sender(dv_s.at[j, trow(p)], dvr.at[me, j], dv_ss.at[j, i], dv_rs.at[j, i], (p, mine)))
+            go(remote(dv_s.at[j, trow(p)], dvr.at[me, j], dv_rs.at[j, i], (p, mine)))
         dvr[me, j] = dv_s[j, trow(me), :]
 
     def one_pair(j):
         for i, p in enumerate(peers):
-            r = vog_all.at[j, :, trow(p)]
-            sender(vog_src.at[i, j], r, vog_ss.at[j, i], vog_rs.at[j, i], (p, mine)).wait_recv()
+            r = vog_all.at[:, trow(p), j * pw : (j + 1) * pw]
+            arrive(remote(r, r, vog_rs.at[j, i], (p, mine)))
         if j == 0:
             go(other_aside())
-        vt_s[...] = vog_all[j, 0].T
-        ogt_s[...] = vog_all[j, 1].T
-        for hh in range(2):
-            head_back(hh, 2 * j + hh, cos, sin, lams[2 * j + hh], qt_s, kt_s, p_s, vt_s, ogt_s, dvt_s, dk_s, bt_s)
+        vt_s[...] = vog_all[0, :, j * pw : (j + 1) * pw].T
+        ogt_s[...] = vog_all[1, :, j * pw : (j + 1) * pw].T
+        pair_back(2 * j, cos, sin, lams[2 * j : 2 * j + 2], qt_s, kt_s, p_s, vt_s, ogt_s, dvt_s, dk_s, bt_s)
         back_m[j] = bt_s[...].T
         for a, to in enumerate((0, 1)):
             for b, p in enumerate((peers[to], peers[2])):
-                go(sender(back_m.at[j, trow(p)], back_x.at[a, j, b], bx_ss.at[a, j, b], bx_rs.at[a, j, b], (xp, yp)[to]))
+                go(remote(back_m.at[j, trow(p)], back_x.at[a, j, b], bx_rs.at[a, j, b], (xp, yp)[to]))
+
+        if j:
+            merge(j - 1)
 
         def weight_part(c):
             return dot(bt_s[...], tok_all[:, lanes(c, nz * wr)])
@@ -687,51 +716,52 @@
         part = weight_part(1 - core)
         for zz in range(nz):
             sib_s[j, zz] = part[:, zz * wr : (zz + 1) * wr].astype(BF16)
-        for zz in range(nz):
-            go(sender(sib_s.at[j, zz], sib_r.at[j, zz], c_ss.at[j, zz], c_rs.at[j, zz], sib))
+        go(remote(sib_s.at[j], sib_r.at[j], c_rs.at[j], sib))
         part = weight_part(core)
         for zz in range(nz):
             own_s[j, zz] = part[:, zz * wr : (zz + 1) * wr]
         dv_s[j] = dvt_s[...].T.astype(BF16)
         values_start(j)
-        if j:
-            merge(j - 1)
+
+    def shares(j):
+        arrive(remote(sib_s.at[j], sib_r.at[j], c_rs.at[j], sib))
         for i in range(nz):
-            sender(sib_s.at[j, i], sib_r.at[j, i], c_ss.at[j, i], c_rs.at[j, i], sib).wait_recv()
             own_s[j, i] = own_s[j, i] + sib_r[j, i].astype(F32)
         for i in range(nz - 1):
             wz_s[j, i] = own_s[j, order[i]].astype(BF16)
-        go(sender(wz_s.at[j, 2], wz_m.at[j], g_ss.at[j, 2], m_rs.at[j], (me, 2 * order[1] + core)), outer)
+        go(remote(wz_s.at[j, 2], wz_m.at[j], m_rs.at[j], (me, 2 * order[1] + core)), outer)
         go(z_share(j, 0), outer)
         go(z_share(j, 2), inner)
         go(z_share(j, 1))
 
     def z_share(j, i):
-        return sender(wz_s.at[j, i], wz_r.at[j, i], g_ss.at[j, i], g_rs.at[j, i], (me, 2 * order[i] + core))
+        return remote(wz_s.at[j, i], wz_r.at[j, i], g_rs.at[j, i], (me, 2 * order[i] + core))
 
     def merge(j):
-        c = z_share(j, 0)
+        copy = ready(z_share(j, 0), inner)
 
         @pl.when(inner)
         def _():
-            sender(wz_m.at[j], wz_m.at[j], g_ss.at[j, 0], m_rs.at[j], sib).wait_recv()
+            arrive(remote(wz_m.at[j], wz_m.at[j], m_rs.at[j], sib))
             wz_s[j, 0] = (own_s[j, far] + wz_m[j].astype(F32)).astype(BF16)
-            c.start()
-
-        sends.append((c, inner))
-
+            copy.start()
+
+    scores(0)
+    flush(10)
+    for j in range(1, pairs):
+        vog_start(j)
+        scores(j)
     for j in range(pairs):
-        scores(j)
-        if j == 0:
-            for jj in range(1, pairs):
-                vog_start(jj)
         one_pair(j)
         if j == 0:
+            done = len(sends)
+        shares(j)
+        if j == 0:
             other_step(near[0])
 
     def back_wait(a, j, b):
         r = back_x.at[a, j, b]
-        sender(r, r, bx_ss.at[a, j, b], bx_rs.at[a, j, b], sib).wait_recv()
+        arrive(remote(r, r, bx_rs.at[a, j, b], sib))
 
     def token_part(who, a, b, parts):
         n = slice(a * nz * wr, (a + 1) * nz * wr)
@@ -753,22 +783,23 @@
                 back_wait(a, j, b)
     for a in range(2):
         tacc[a] = token_part(peers[1 - a], a, 1, early)
+    flush(done)
     ty = {}
     for a in range(2):
         back_wait(a, pairs - 1, 1)
         tbuf[a] = (tacc[a] + token_part(peers[1 - a], a, 1, late)).astype(BF16)
         for h in range(2):
             r = pl.ds(h * half, half)
-            ty[a, h] = go(sender(tbuf.at[a, r], trecv.at[a, r], ty_ss.at[a, h], ty_rs.at[a, h], (yp, xp)[a]))
+            ty[a, h] = go(remote(tbuf.at[a, r], trecv.at[a, r], ty_rs.at[a, h], (yp, xp)[a]))
 
     def weights_end(j):
         @pl.when(inner)
         def _():
-            z_share(j, 2).wait_recv()
+            arrive(z_share(j, 2))
             own_s[j, z] = own_s[j, z] + wz_r[j, 2].astype(F32)
 
-        z_share(j, 0).wait_recv()
-        z_share(j, 1).wait_recv()
+        arrive(z_share(j, 0))
+        arrive(z_share(j, 1))
         total = own_s[j, z] + wz_r[j, 0].astype(F32) + wz_r[j, 1].astype(F32)
         wg_r[me, j] = total.T.astype(BF16)
         for h, k, to in ((0, 0, xp), (1, 1, yp), (1, 2, xp), (0, 3, yp)):
@@ -778,12 +809,12 @@
 
     def ag(owner, j, h, k, to):
         r = wg_r.at[owner, j, pl.ds(h * wh, wh)]
-        return sender(r, r, ag_ss.at[j, k], ag_rs.at[j, k], to)
+        return remote(r, r, ag_rs.at[j, k], to)
 
     def weights_relay(j):
-        ag(peers[0], j, 0, 0, xp).wait_recv()
+        arrive(ag(peers[0], j, 0, 0, xp))
         go(ag(peers[0], j, 0, 4, yp))
-        ag(peers[1], j, 1, 1, yp).wait_recv()
+        arrive(ag(peers[1], j, 1, 1, yp))
         go(ag(peers[1], j, 1, 5, xp))
 
     merge(pairs - 1)
@@ -796,7 +827,9 @@
         weights_end(j)
     for h in range(2):
         for a in range(2):
-            ty[a, h].wait_recv()
+            arrive(ty[a, h])
+            if h == 1 and a == 1:
+                flush(len(sends) - 4 * pairs)
             r = slice(h * half, (h + 1) * half)
             total = (tacc[a, r] + trecv[a, r].astype(F32)).astype(BF16)
             for zz in range(nz):
@@ -806,14 +839,10 @@
     for j in range(pairs):
         for i, p in enumerate(peers):
             r = dvr.at[p, j]
-            sender(r, r, dv_ss.at[j, i], dv_rs.at[j, i], xp).wait_recv()
+            arrive(remote(r, r, dv_rs.at[j, i], xp))
         for owner, h, k in ((peers[0], 1, 2), (peers[1], 0, 3), (peers[2], 0, 4), (peers[2], 1, 5)):
-            ag(owner, j, h, k, xp).wait_recv()
-    for c, cond in sends:
-        if cond is None:
-            c.wait_send()
-        else:
-            pl.when(cond)(c.wait_send)
+            arrive(ag(owner, j, h, k, xp))
+    flush(len(sends))
 
 
 def finish_kernel(factor, tg, dvr, wg, tg_out, dv_out, qg_out, kg_out, dv_s, qg, kg, sem):
@@ -867,7 +896,7 @@
         scratch_shapes=[
             pltpu.SMEM(lam.shape, F32), V(rot.shape, F32),
             V((seq, width), BF16), V((width, 2 * pairs * pw), BF16), V((width, 2 * pairs * pw), BF16),
-            V((seq, 2 * pairs * pw), F32), V((sp - 1, pairs, 2, rows, pw), BF16), V((pairs, 2, seq, pw), BF16),
+            V((seq, 2 * pairs * pw), F32), V((sp - 1, 2, rows, pairs * pw), BF16), V((2, seq, pairs * pw), BF16),
             V((2 * pairs, 2 * DQK, seq), BF16), V((2 * pairs, 2 * DQK, seq), BF16), V((2 * pairs, 2, seq, seq), F32),
             V((pw, seq), BF16), V((pw, seq), BF16), V((pw, seq), F32), V((pw, seq), F32), V((2 * pw, seq), BF16),
             V((pairs, seq, 2 * pw), BF16), V((2, pairs, 2, rows, 2 * pw), BF16),
@@ -875,12 +904,8 @@
             V((pairs, nz, 2 * pw, wr), BF16), V((pairs, nz, 2 * pw, wr), BF16), V((pairs, nz, 2 * pw, wr), F32),
             V((pairs, nz - 1, 2 * pw, wr), BF16), V((pairs, nz - 1, 2 * pw, wr), BF16), V((pairs, 2 * pw, wr), BF16),
             V((2, rows, nz * wr), BF16), V((2, rows, nz * wr), BF16), V((2, rows, nz * wr), F32),
-            dma((2 + dp + 8 * pairs + 2 * sp * pairs,)),
-            dma((6,)), dma((6,)), dma((pairs, sp - 1)), dma((pairs, sp - 1)),
-            dma((2, 4)), dma((2, nz)), dma((2, nz)), dma((2, nz)),
-            dma((2, pairs, 2)), dma((2, pairs, 2)), dma((pairs, sp - 1)), dma((pairs, sp - 1)),
-            dma((pairs, nz)), dma((pairs, nz)), dma((pairs, nz - 1)), dma((pairs, nz - 1)), dma((pairs,)),
-            dma((pairs, 6)), dma((pairs, 6)), dma((2, 2)), dma((2, 2)),
+            dma((44,)), dma((6,)), dma((pairs, sp - 1)), dma((2, nz)), dma((2, nz)), dma((2, pairs, 2)),
+            dma((pairs, sp - 1)), dma((pairs,)), dma((pairs, nz - 1)), dma((pairs,)), dma((pairs, 6)), dma((2, 2)),
         ],
         compiler_params=pltpu.CompilerParams(
             vmem_limit_bytes=56 * 1024 * 1024, collective_id=2, has_side_effects=True

time: 72.8 us -> 69.6 us (0.956)
  Pallas kernels: 71.9 us -> 68.6 us
    pallas_call x1, Pallas kernels: 70.2 us -> 67 us  [fused(): pl.pallas_call(functools.partial(fused_kernel, sp, dp, pairs), out_shape=...]
where the time goes in v4:
time: 69.6 us; the launch traced here: 69.4 us
  Pallas kernels  68.6 us (99%)
  between operations  0.8 us (1%)
    pallas_call x1, Pallas kernels, fused(): pl.pallas_call(functools.partial(fused_kernel, sp, dp, pairs), out_shape=...  67 us
    pallas_call x1, Pallas kernels, fused(): pl.pallas_call(functools.partial(finish_kernel, factor), out_shape=(jax.S...  1.67 us

profile of v4, /device:TPU:0, one launch (start us, length us, event | category | flops | bytes accessed | tf_op | source)
XLA Modules:
  0.0 69.4 jit_solution(12979533062746247861)
XLA Ops:
  0.6 67.0 %fused.1 = (bf16[160,2048]{1,0:T(8,128)(2,1)S(1)}, bf16[4,2,160,128]{3,2,1,0:T(8,128)(2,1)S(1)}, bf16[4,2,256,256]{3,2,1,0:T(8,128)(2,1)S(1)}) custom-call(f32[16]{0:T(128)} %lam_in.1, f32[32,640]{1,0:T(8,128)} %constant.2.clone.rot_in, bf16[160,2048]{1,0:T(8,128)(2,1)} %bitcast.5, bf16[160,1024]{1,0:T(8,128)(2,1)} %bitcast.6, bf16[160,1024]{1,0:T(8,128)(2,1)} %bitcast.7, ...), custom_call_target="tpu_custom_call" | custom-call | tf_op jit(solution)/shard_map/fused/pallas_call | solution.py:887
  67.6 1.7 %finish.1 = (bf16[160,2048]{1,0:T(8,128)(2,1)}, bf16[160,1024]{1,0:T(8,128)(2,1)}, f32[256,1024]{1,0:T(8,128)}, f32[256,1024]{1,0:T(8,128)}) custom-call(bf16[160,2048]{1,0:T(8,128)(2,1)S(1)} %get-tuple-element.11.tg, bf16[4,2,160,128]{3,2,1,0:T(8,128)(2,1)S(1)} %get-tuple-element.12.dvr, bf16[4,2,256,256]{3,2,1,0:T(8,128)(2,1)S(1)} %get-tuple-element.13.wg), custom_call_target="tpu_custom_call" | custom-call | tf_op jit(solution)/shard_map/finish/pallas_call | solution.py:915

commit v5 on v4

--- a/solution.py
+++ b/solution.py
@@ -430,7 +430,7 @@
     return jnp.asarray(np.concatenate([np.cos(wide), np.sin(wide)]).astype(np.float32))
 
 
-def head_scores(hh, cos, sin, q, k_in, qt_s, kt_s, p_s, lam):
+def head_scores(hh, cos, sin, q, k_in, qt_s, kt_s, p_s, r_s, lam):
     seq = cos.shape[1]
     scale = math.log2(math.e) / math.sqrt(DQK)
     step = 256
@@ -454,10 +454,11 @@
             s = jnp.concatenate([s[:t0], diag], axis=0) if t0 else diag
             e = jnp.exp2((s - jnp.max(s, axis=0, keepdims=True)) * scale)
             r = 1.0 / jnp.sum(e, axis=0, keepdims=True)
-            p_s[hh, m, :end, t0:end] = e * (r if m == 0 else r * -lam)
-
-
-def pair_back(h0, cos, sin, lams, qt_s, kt_s, p_s, vt_s, ogt_s, dvt_s, dk_s, bt_s):
+            p_s[hh, m, :end, t0:end] = e
+            r_s[hh, m : m + 1, t0:end] = r if m == 0 else r * -lam
+
+
+def pair_back(h0, cos, sin, lams, qt_s, kt_s, p_s, r_s, vt_s, ogt_s, dvt_s, dk_s, bt_s):
     seq = cos.shape[1]
     hw = 2 * DQK
     ve = vt_s.shape[0] // 2
@@ -472,7 +473,8 @@
     mix, ho, ob, g1, g2 = {}, {}, {}, {}, {}
     for w in work:
         hh, t0, end = w
-        mix[w] = (p_s[h0 + hh, 0, :end, t0:end] + p_s[h0 + hh, 1, :end, t0:end]).astype(BF16)
+        r1, r2 = r_s[h0 + hh, 0:1, t0:end], r_s[h0 + hh, 1:2, t0:end]
+        mix[w] = (p_s[h0 + hh, 0, :end, t0:end] * r1 + p_s[h0 + hh, 1, :end, t0:end] * r2).astype(BF16)
         ho[w] = dot(vt[hh][:, :end], mix[w])
     for w in work:
         hh, t0, end = w
@@ -484,8 +486,10 @@
         hh, t0, end = w
         mg = dot(v[hh][:end], ob[w])
         p1, p2 = p_s[h0 + hh, 0, :end, t0:end], p_s[h0 + hh, 1, :end, t0:end]
-        g1[w] = (p1 * (mg - jnp.sum(mg * p1, axis=0, keepdims=True))).astype(BF16)
-        g2[w] = (p2 * (mg + jnp.sum(mg * p2, axis=0, keepdims=True) * (1.0 / lams[hh]))).astype(BF16)
+        r1, r2 = r_s[h0 + hh, 0:1, t0:end], r_s[h0 + hh, 1:2, t0:end]
+        m1, m2 = mg * r1, mg * r2
+        g1[w] = (p1 * (m1 - jnp.sum(m1 * p1, axis=0, keepdims=True) * r1)).astype(BF16)
+        g2[w] = (p2 * (m2 + jnp.sum(m2 * p2, axis=0, keepdims=True) * (r2 / lams[hh]))).astype(BF16)
         q_b, kt = qt_s[h0 + hh, :, t0:end], kt_s[h0 + hh]
         dq = jnp.concatenate([dot(kt[:DQK, :end], g1[w]), dot(kt[DQK:, :end], g2[w])], axis=0)
         bt_s[rows[hh], t0:end] = rotate_rows(dq, cb[:, t0:end], sb[:, t0:end]).astype(BF16)
@@ -502,7 +506,7 @@
 
 def fused_kernel(sp, dp, pairs, lam_in, rot_in, tok_in, v_in, og_in, wq_in, wk_in,
                  tg_out, dvr, wg_r,
-                 lam_ref, rot_ref, tok_all, w1, w2, qk_s, vog_src, vog_all, qt_s, kt_s, p_s,
+                 lam_ref, rot_ref, tok_all, w1, w2, qk_s, vog_src, vog_all, qt_s, kt_s, p_s, r_s,
                  vt_s, ogt_s, dvt_s, dk_s, bt_s, back_m, back_x,
                  dv_s, sib_s, sib_r, own_s, wz_s, wz_r, wz_m, tbuf, trecv, tacc,
                  pool, tok_rs, vog_rs, z_rs, s_rs, bx_rs, dv_rs, c_rs, g_rs, m_rs, ag_rs, ty_rs):
@@ -644,10 +648,11 @@
     loaded(l_w1)
     z_start()
     l_vog = []
-    for n, src in enumerate((v_in, og_in)):
-        for i, p in enumerate(peers):
-            l_vog.append(load(src.at[:, lanes(p, pairs * pw)], vog_src.at[i, n]))
-        l_vog.append(load(src.at[:, lanes(me, pairs * pw)], vog_all.at[n, trow(me)]))
+    for j in range(pairs):
+        for n, src in enumerate((v_in, og_in)):
+            for i, p in enumerate(peers):
+                l_vog.append(load(src.at[:, lanes(p * pairs + j, pw)], vog_src.at[i, j, n]))
+            l_vog.append(load(src.at[:, lanes(me * pairs + j, pw)], vog_all.at[j, n, trow(me)]))
     l_w2 = load_weights(w2, jnp.where(core == 0, peers[0], peers[1]))
     l_rot = [load(rot_in, rot_ref), load(lam_in, lam_ref)]
     loaded(l_w2 + l_vog + l_rot)
@@ -660,9 +665,7 @@
 
     def vog_start(j):
         for i in range(sp - 1):
-            n = slice(j * pw, (j + 1) * pw)
-            dst = vog_all.at[:, trow(me), n]
-            go(remote(vog_src.at[i, :, :, n], dst, vog_rs.at[j, i], (peers[i], mine)))
+            go(remote(vog_src.at[i, j], vog_all.at[j, :, trow(me)], vog_rs.at[j, i], (peers[i], mine)))
 
     vog_start(0)
     z_step(0)
@@ -686,7 +689,7 @@
         for hh in range(2):
             r = slice(hh * hw, (hh + 1) * hw)
             h = 2 * j + hh
-            head_scores(h, cos, sin, qk[0][r], qk[1][r], qt_s, kt_s, p_s, lams[h])
+            head_scores(h, cos, sin, qk[0][r], qk[1][r], qt_s, kt_s, p_s, r_s, lams[h])
 
     def values_start(j):
         for i, p in enumerate(peers):
@@ -695,13 +698,13 @@
 
     def one_pair(j):
         for i, p in enumerate(peers):
-            r = vog_all.at[:, trow(p), j * pw : (j + 1) * pw]
+            r = vog_all.at[j, :, trow(p)]
             arrive(remote(r, r, vog_rs.at[j, i], (p, mine)))
         if j == 0:
             go(other_aside())
-        vt_s[...] = vog_all[0, :, j * pw : (j + 1) * pw].T
-        ogt_s[...] = vog_all[1, :, j * pw : (j + 1) * pw].T
-        pair_back(2 * j, cos, sin, lams[2 * j : 2 * j + 2], qt_s, kt_s, p_s, vt_s, ogt_s, dvt_s, dk_s, bt_s)
+        vt_s[...] = vog_all[j, 0].T
+        ogt_s[...] = vog_all[j, 1].T
+        pair_back(2 * j, cos, sin, lams[2 * j : 2 * j + 2], qt_s, kt_s, p_s, r_s, vt_s, ogt_s, dvt_s, dk_s, bt_s)
         back_m[j] = bt_s[...].T
         for a, to in enumerate((0, 1)):
             for b, p in enumerate((peers[to], peers[2])):
@@ -896,8 +899,8 @@
         scratch_shapes=[
             pltpu.SMEM(lam.shape, F32), V(rot.shape, F32),
             V((seq, width), BF16), V((width, 2 * pairs * pw), BF16), V((width, 2 * pairs * pw), BF16),
-            V((seq, 2 * pairs * pw), F32), V((sp - 1, 2, rows, pairs * pw), BF16), V((2, seq, pairs * pw), BF16),
-            V((2 * pairs, 2 * DQK, seq), BF16), V((2 * pairs, 2 * DQK, seq), BF16), V((2 * pairs, 2, seq, seq), F32),
+            V((seq, 2 * pairs * pw), F32), V((sp - 1, pairs, 2, rows, pw), BF16), V((pairs, 2, seq, pw), BF16),
+            V((2 * pairs, 2 * DQK, seq), BF16), V((2 * pairs, 2 * DQK, seq), BF16), V((2 * pairs, 2, seq, seq), F32), V((2 * pairs, 2, seq), F32),
             V((pw, seq), BF16), V((pw, seq), BF16), V((pw, seq), F32), V((pw, seq), F32), V((2 * pw, seq), BF16),
             V((pairs, seq, 2 * pw), BF16), V((2, pairs, 2, rows, 2 * pw), BF16),
             V((pairs, seq, pw), BF16),

time: 69.6 us -> 69.7 us (level)
  no operation moved by 1% of the time
where the time goes in v5:
time: 69.7 us; the launch traced here: 69.5 us
  Pallas kernels  68.7 us (99%)
  between operations  0.8 us (1%)
    pallas_call x1, Pallas kernels, fused(): pl.pallas_call(functools.partial(fused_kernel, sp, dp, pairs), out_shape=...  67 us
    pallas_call x1, Pallas kernels, fused(): pl.pallas_call(functools.partial(finish_kernel, factor), out_shape=(jax.S...  1.67 us

profile of v5, /device:TPU:0, one launch (start us, length us, event | category | flops | bytes accessed | tf_op | source)
XLA Modules:
  0.0 69.5 jit_solution(3801311000457812588)
XLA Ops:
  0.6 67.0 %fused.1 = (bf16[160,2048]{1,0:T(8,128)(2,1)S(1)}, bf16[4,2,160,128]{3,2,1,0:T(8,128)(2,1)S(1)}, bf16[4,2,256,256]{3,2,1,0:T(8,128)(2,1)S(1)}) custom-call(f32[16]{0:T(128)} %lam_in.1, f32[32,640]{1,0:T(8,128)} %constant.2.clone.rot_in, bf16[160,2048]{1,0:T(8,128)(2,1)} %bitcast.5, bf16[160,1024]{1,0:T(8,128)(2,1)} %bitcast.6, bf16[160,1024]{1,0:T(8,128)(2,1)} %bitcast.7, ...), custom_call_target="tpu_custom_call" | custom-call | tf_op jit(solution)/shard_map/fused/pallas_call | solution.py:890
  67.6 1.7 %finish.1 = (bf16[160,2048]{1,0:T(8,128)(2,1)}, bf16[160,1024]{1,0:T(8,128)(2,1)}, f32[256,1024]{1,0:T(8,128)}, f32[256,1024]{1,0:T(8,128)}) custom-call(bf16[160,2048]{1,0:T(8,128)(2,1)S(1)} %get-tuple-element.11.tg, bf16[4,2,160,128]{3,2,1,0:T(8,128)(2,1)S(1)} %get-tuple-element.12.dvr, bf16[4,2,256,256]{3,2,1,0:T(8,128)(2,1)S(1)} %get-tuple-element.13.wg), custom_call_target="tpu_custom_call" | custom-call | tf_op jit(solution)/shard_map/finish/pallas_call | solution.py:918
